TPU v7x, 256 devices: a whole 4x4x8 slice. The times are simulated.
256 devices in a mesh: ep: 32 (over z, x), tp: 8 (over y, core).
Axes of the slice: x: 4, y: 4, z: 8, core: 2. Of those that a mesh axis runs over, the one named last changes fastest.
Arguments:
- resid: bfloat16 [1024, 2048], P('ep'), may hold values from -6 to 6
- norm_gain: bfloat16 [2048], replicated, may hold values from 0.099609375 to 1.8984375
- w_query: bfloat16 [2048, 1024], P(None, 'tp'), may hold values from -0.125 to 0.125
- w_key: bfloat16 [2048, 1024], P(None, 'tp'), may hold values from -0.125 to 0.125
- w_value: bfloat16 [2048, 1024], P(None, 'tp'), may hold values from -0.125 to 0.125
- w_gate: bfloat16 [2048, 1024], P(None, 'tp'), may hold values from -0.125 to 0.125
- head_gain: bfloat16 [1024], P('tp'), may hold values from 0.099609375 to 1.8984375
- w_output: bfloat16 [1024, 2048], P('tp'), may hold values from -0.1875 to 0.1875
- state: float32 [1024, 8, 128, 128], P('ep', 'tp'), may hold values from -0.6 to 0.6
- positions: int32 [1024], P('ep'), may hold values from 1024 to 8191
- ffn_gain: bfloat16 [2048], replicated, may hold values from 0.099609375 to 1.8984375
- w_mix: bfloat16 [2048], replicated, may hold values from -0.125 to 0.125
- dense_gate: bfloat16 [2048, 5632], P('tp', 'ep'), may hold values from -0.125 to 0.125
- dense_up: bfloat16 [2048, 5632], P('tp', 'ep'), may hold values from -0.125 to 0.125
- dense_down: bfloat16 [5632, 2048], P('ep', 'tp'), may hold values from -0.15625 to 0.15625
- routes: int32 [1024, 2], P('ep'), may hold values from 0 to 31, all different within a row; in each aligned block of 32 rows (0 to 31, 32 to 63, ...) at most 4 rows name the same one
- route_weight: bfloat16 [1024, 2], P('ep'), may hold values from 0.19921875 to 1
- expert_gate: bfloat16 [32, 2048, 4096], P('ep', None, 'tp'), may hold values from -0.125 to 0.125
- expert_up: bfloat16 [32, 2048, 4096], P('ep', None, 'tp'), may hold values from -0.125 to 0.125
- expert_down: bfloat16 [32, 4096, 2048], P('ep', 'tp'), may hold values from -0.09375 to 0.09375
Outputs:
- final: bfloat16 [1024, 2048], P('ep', 'tp')
- new_state: float32 [1024, 8, 128, 128], P('ep', 'tp')
Inputs may be any that keep to these rules, and one draw needn't show every extreme that they name: `routes`: each row names 2 different experts; in the rows of one index of ep no expert is named by more than 4 rows, a bound that some block reaches; every expert is named by some row.
All inputs are finite; a program needn't handle non-finite values.
Results may differ from a plain program's by a relative error of at most 0.018.
Values may be sent and summed in bfloat16 or wider, within the bound.
A program may use at most 64 MiB of HBM per device.

v0:
```python
import jax
import jax.numpy as jnp
from jax import lax
from jax.sharding import PartitionSpec as P

EPSILON = 1e-06
THETA = 10000.0


def split_up(value, dim, length):
    before, after = (value.shape[:dim], value.shape[dim + 1 :])
    return jnp.moveaxis(value.reshape(*before, length, -1, *after), dim, 0)


def sent_and_summed(value, axis, dim):
    tiles = split_up(value, dim, lax.axis_size(axis))
    arrived = lax.all_to_all(tiles, axis, split_axis=0, concat_axis=0, tiled=True)
    return arrived.astype(jnp.float32).sum(axis=0)


def copy_for_each(value, axis):
    copies = jnp.broadcast_to(value, (lax.axis_size(axis), *value.shape))
    return lax.all_to_all(copies, axis, split_axis=0, concat_axis=0, tiled=True)


def of_everyone(value, axis):
    everything = copy_for_each(value, axis)
    return jnp.sum(everything.astype(jnp.float32), axis=0)


def in_order(tiles, dim):
    dims = list(tiles.shape[1:])
    dims[dim] *= tiles.shape[0]
    return jnp.moveaxis(tiles, 0, dim).reshape(dims)


def gather_directly(value, axis, dim):
    tiles = copy_for_each(value, axis)
    return in_order(tiles, dim)


def packed_total(arrays, axis):
    flat, at, outs = (jnp.concatenate([a.reshape(-1) for a in arrays]), 0, [])
    running = lax.psum(flat, axis)
    for a in arrays:
        outs.append(running[at : at + a.size].reshape(a.shape))
        at += a.size
    return tuple(outs)


def rms_norm(inputs, scaling):
    square = jnp.mean(inputs * inputs, axis=-1, keepdims=True)
    return inputs * lax.rsqrt(square + EPSILON) * scaling.astype(jnp.float32)


def rotate(inputs, places):
    halfway = inputs.shape[-1] // 2
    inverse = THETA ** (-jnp.arange(halfway, dtype=jnp.float32) / halfway)
    angles = places.astype(jnp.float32)[:, None] * inverse[None, :]
    cosine = jnp.cos(angles)[:, None, :]
    sine_of = jnp.sin(angles)[:, None, :]
    former = inputs[..., :halfway]
    latter = inputs[..., halfway:]
    return jnp.concatenate(
        [former * cosine - latter * sine_of, former * sine_of + latter * cosine], axis=-1
    )


def retain(queries, keys_in, values_in, gating, memory, places, head_first, head_gain):
    seqs_here = queries.shape[0]
    heads_here = memory.shape[1]
    head_size = memory.shape[2]
    head_shape = (seqs_here, heads_here, head_size)
    query_rot = rotate(queries.astype(jnp.float32).reshape(head_shape), places)
    key_rot = rotate(keys_in.astype(jnp.float32).reshape(head_shape), places) * head_size ** (-0.5)
    value_heads = values_in.astype(jnp.float32).reshape(head_shape)
    head_index = head_first + jnp.arange(heads_here, dtype=jnp.float32)
    decays = 1.0 - jnp.exp2(-1.0 - 1.5 * head_index)
    within = jnp.sum(query_rot * key_rot, axis=-1, keepdims=True) * value_heads
    carried = jnp.einsum("shd,shde->she", query_rot, memory) * decays[None, :, None]
    mixture = within + carried
    new_memory = (
        decays[None, :, None, None] * memory + key_rot[:, :, :, None] * value_heads[:, :, None, :]
    )
    centre = jnp.mean(mixture, axis=-1, keepdims=True)
    spread = jnp.mean(jnp.square(mixture - centre), axis=-1, keepdims=True)
    normed = ((mixture - centre) * lax.rsqrt(spread + EPSILON)).reshape(
        seqs_here, heads_here * head_size
    )
    normed = normed * head_gain.astype(jnp.float32)
    output = (jax.nn.silu(gating.astype(jnp.float32)) * normed).astype(jnp.bfloat16)
    return (output, new_memory)


def expert_hidden(chosen, gate_weight, up_weight):
    gate_value = jnp.dot(chosen, gate_weight, preferred_element_type=jnp.float32)
    up_value = jnp.dot(chosen, up_weight, preferred_element_type=jnp.float32)
    return (jax.nn.silu(gate_value) * up_value).astype(jnp.bfloat16)


def padded_experts(
    normed_mid, routes, route_weight, expert_gate, expert_up, expert_down, capacity, experts_all
):
    seq_dev, model_width = normed_mid.shape
    top_count = routes.shape[1]
    flat_ids = routes.reshape(-1)
    expert_ids = jnp.arange(experts_all, dtype=jnp.int32)
    onehot = (flat_ids[:, None] == expert_ids[None, :]).astype(jnp.int32)
    ranks = jnp.sum((jnp.cumsum(onehot, axis=0) - 1) * onehot, axis=1)
    slot_ids = flat_ids * capacity + ranks
    slot_range = jnp.arange(experts_all * capacity, dtype=jnp.int32)
    dispatch = (slot_range[:, None] == slot_ids[None, :]).astype(jnp.bfloat16)
    repeated = jnp.repeat(normed_mid, top_count, axis=0)
    outgoing = jnp.dot(dispatch, repeated, preferred_element_type=jnp.float32).astype(jnp.bfloat16)
    outgoing = outgoing.reshape(experts_all, capacity, model_width)
    arrived = lax.all_to_all(outgoing, "ep", split_axis=0, concat_axis=0, tiled=True)
    sources = arrived.shape[0]
    items = arrived.shape[1]
    hidden_e = expert_hidden(
        arrived.reshape(sources * items, model_width), expert_gate[0], expert_up[0]
    )
    partial_value = jnp.dot(hidden_e, expert_down[0], preferred_element_type=jnp.float32)
    summed = sent_and_summed(partial_value.astype(jnp.bfloat16), "tp", 1).astype(jnp.bfloat16)
    returned = lax.all_to_all(
        summed.reshape(sources, items, summed.shape[1]),
        "ep",
        split_axis=0,
        concat_axis=0,
        tiled=True,
    )
    flat_back = returned.reshape(experts_all * capacity, returned.shape[2])
    weighted = flat_back[slot_ids].astype(jnp.float32) * route_weight.reshape(-1)[:, None].astype(
        jnp.float32
    )
    return jnp.sum(weighted.reshape(seq_dev, top_count, weighted.shape[1]), axis=1)


def per_device(
    resid,
    norm_gain,
    w_query,
    w_key,
    w_value,
    w_gate,
    head_gain,
    w_output,
    state,
    positions,
    ffn_gain,
    w_mix,
    dense_gate,
    dense_up,
    dense_down,
    routes,
    route_weight,
    expert_gate,
    expert_up,
    expert_down,
):
    seq_dev = resid.shape[0]
    model_width = resid.shape[1]
    tp_count = lax.axis_size("tp")
    ep_count = lax.axis_size("ep")
    model_tp = model_width // tp_count
    tp_index = lax.axis_index("tp")
    normed_in = rms_norm(resid.astype(jnp.float32), norm_gain).astype(jnp.bfloat16)

    def project(weight):
        return jnp.dot(normed_in, weight, preferred_element_type=jnp.float32).astype(jnp.bfloat16)

    heads_here = state.shape[1]
    head_first = (tp_index * heads_here).astype(jnp.float32)
    retained, new_state = retain(
        project(w_query),
        project(w_key),
        project(w_value),
        project(w_gate),
        state,
        positions,
        head_first,
        head_gain,
    )
    partial_value = jnp.dot(retained, w_output, preferred_element_type=jnp.float32)
    attention = of_everyone(partial_value.astype(jnp.bfloat16), "tp").astype(jnp.float32)
    middle = resid.astype(jnp.float32) + attention
    normed_mid = rms_norm(middle, ffn_gain).astype(jnp.bfloat16)
    mixing = jax.nn.sigmoid(jnp.dot(normed_mid, w_mix[:, None], preferred_element_type=jnp.float32))

    def own_columns(matrix):
        return lax.dynamic_slice_in_dim(matrix, tp_index * model_tp, model_tp, 1)

    top_count = routes.shape[1]
    capacity = max(2, 2 * seq_dev * top_count // ep_count)
    dense_rows = gather_directly(own_columns(normed_mid), "ep", 0)
    moe_out = padded_experts(
        normed_mid, routes, route_weight, expert_gate, expert_up, expert_down, capacity, ep_count
    )
    gate_part = jnp.dot(dense_rows, dense_gate, preferred_element_type=jnp.float32)
    up_part = jnp.dot(dense_rows, dense_up, preferred_element_type=jnp.float32)
    gate_sum, up_sum = tuple(
        (
            part.astype(jnp.float32)
            for part in packed_total(
                (gate_part.astype(jnp.bfloat16), up_part.astype(jnp.bfloat16)), "tp"
            )
        )
    )
    dense_hidden = (jax.nn.silu(gate_sum) * up_sum).astype(jnp.bfloat16)
    dense_out = sent_and_summed(
        jnp.dot(dense_hidden, dense_down, preferred_element_type=jnp.float32).astype(jnp.bfloat16),
        "ep",
        0,
    )
    final = (own_columns(middle) + moe_out + mixing * dense_out).astype(jnp.bfloat16)
    return (final, new_state)


def solution(mesh):
    in_specs = (
        P("ep", None),
        P(),
        P(None, "tp"),
        P(None, "tp"),
        P(None, "tp"),
        P(None, "tp"),
        P("tp"),
        P("tp", None),
        P("ep", "tp", None, None),
        P("ep"),
        P(),
        P(),
        P("tp", "ep"),
        P("tp", "ep"),
        P("ep", "tp"),
        P("ep", None),
        P("ep", None),
        P("ep", None, "tp"),
        P("ep", None, "tp"),
        P("ep", "tp", None),
    )
    out_specs = (P("ep", "tp"), P("ep", "tp", None, None))
    return jax.shard_map(
        per_device, mesh=mesh, in_specs=in_specs, out_specs=out_specs, check_vma=False
    )
```

profile of v0, /device:TPU:24, one launch (start us, length us, event | category | flops | bytes accessed | tf_op | source)
XLA Modules:
  0.0 206.2 jit_solution(7254978397219586404)
XLA Ops:
  7.3 0.8 convert_element_type.126
  8.1 0.7 convert_element_type.121
  8.7 1.0 fusion.25
  9.8 0.7 convert_element_type.116
  10.5 1.4 fusion.18
  11.9 1.4 fusion.20
  13.3 0.1 fusion.44
  13.5 0.2 fusion.49
  13.6 2.0 fusion.66
  15.6 1.0 fusion.65
  16.6 0.2 multiply_reduce_fusion.2
  16.8 1.5 convolution_convert_fusion.2
  18.4 1.1 broadcast_in_dim.6
  19.5 5.4 %all-to-all-start = ((bf16[8,32,2048]{2,1,0:T(8,128)(2,1)}), bf16[8,32,2048]{2,1,0:T(8,128)(2,1)S(1)}, u32[]{:S(2)}, u32[]{:S(2)}) async-start(bf16[8,32,2048]{2,1,0:T(8,128)(2,1)} %broadcast_in_dim.6), calls=%async_computation | async-start | bytes 2097152 | tf_op jit(solution)/shard_map/all_to_all | solution.py:23
  24.9 0.1 copy.36
  25.0 13.7 %all-to-all-done = bf16[8,32,2048]{2,1,0:T(8,128)(2,1)S(1)} async-done(((bf16[8,32,2048]{2,1,0:T(8,128)(2,1)}), bf16[8,32,2048]{2,1,0:T(8,128)(2,1)S(1)}, u32[]{:S(2)}, u32[]{:S(2)}) %all-to-all-start) | async-done | bytes 1048608 | tf_op jit(solution)/shard_map/all_to_all | solution.py:23
  38.7 0.1 convert_reduce_fusion
  38.9 0.1 multiply_reduce_fusion
  39.0 0.7 copy-done.2
  39.8 0.1 multiply_convert_fusion.2
  39.9 0.9 broadcast_in_dim.8
  40.7 10.6 %all-to-all-start.4 = ((bf16[32,32,256]{2,1,0:T(8,128)(2,1)}), bf16[32,32,256]{2,1,0:T(8,128)(2,1)S(1)}, u32[]{:S(2)}, u32[]{:S(2)}) async-start(bf16[32,32,256]{2,1,0:T(8,128)(2,1)} %broadcast_in_dim.8), calls=%async_computation.4 | async-start | bytes 1048576 | tf_op jit(solution)/shard_map/all_to_all | solution.py:23
  51.4 0.1 copy.38
  51.4 0.7 mul.310
  52.1 0.1 reshape.383
  52.3 0.1 reduce_window_sum.11
  52.4 0.2 select_reduce_fusion
  52.6 0.5 copy-done.13
  53.1 0.1 broadcast_in_dim.7
  53.3 0.1 reshape.384
  53.4 0.3 convolution_convert_fusion.1
  53.7 1.0 reshape.385
  54.7 14.1 %all-to-all-done.4 = bf16[32,32,256]{2,1,0:T(8,128)(2,1)S(1)} async-done(((bf16[32,32,256]{2,1,0:T(8,128)(2,1)}), bf16[32,32,256]{2,1,0:T(8,128)(2,1)S(1)}, u32[]{:S(2)}, u32[]{:S(2)}) %all-to-all-start.4) | async-done | bytes 524320 | tf_op jit(solution)/shard_map/all_to_all | solution.py:23
  68.8 4.7 %all-to-all-start.1 = ((bf16[32,4,2048]{2,1,0:T(4,128)(2,1)}), bf16[32,4,2048]{2,1,0:T(4,128)(2,1)S(1)}, u32[]{:S(2)}, u32[]{:S(2)}) async-start(bf16[32,4,2048]{2,1,0:T(4,128)(2,1)} %reshape.385), calls=%async_computation.1 | async-start | bytes 1048576 | tf_op jit(solution)/shard_map/all_to_all | solution.py:116
  73.5 1.2 convolution_convert_fusion.4
  74.7 2.0 convolution_convert_fusion.5
  76.7 1.2 copy.40
  77.9 1.4 reshape.391
  79.3 0.2 copy.41
  79.5 0.7 reshape.392
  80.2 1.9 pad_maximum_fusion
  82.1 8.3 %all-to-all-done.1 = bf16[32,4,2048]{2,1,0:T(4,128)(2,1)S(1)} async-done(((bf16[32,4,2048]{2,1,0:T(4,128)(2,1)}), bf16[32,4,2048]{2,1,0:T(4,128)(2,1)S(1)}, u32[]{:S(2)}, u32[]{:S(2)}) %all-to-all-start.1) | async-done | bytes 524320 | tf_op jit(solution)/shard_map/all_to_all | solution.py:116
  90.5 0.1 reshape.386
  90.6 2.0 fusion.3
  92.6 2.5 %convolution_convert_fusion = bf16[128,2048]{1,0:T(8,128)(2,1)S(1)} fusion(bf16[1,512,2048]{2,1,0:T(8,128)(2,1)S(1)} %copy-done, bf16[128,2048]{1,0:T(8,128)(2,1)S(1)} %reshape.386, bf16[1,2048,512]{2,1,0:T(8,128)(2,1)} %param.38, f32[128,512]{1,0:T(8,128)S(1)} %fusion.3), kind=kOutput, calls=%fused_computation.1 | convolution fusion | flops 537526272 | bytes 5505024 | tf_op jit(solution)/shard_map/dot_general | solution.py:122
  95.1 0.8 copy.46
  95.9 6.1 %all-to-all-start.2 = ((bf16[8,128,256]{2,1,0:T(8,128)(2,1)}), bf16[8,128,256]{2,1,0:T(8,128)(2,1)}, u32[]{:S(2)}, u32[]{:S(2)}) async-start(bf16[8,128,256]{2,1,0:T(8,128)(2,1)} %bitcast.85), calls=%async_computation.2 | async-start | bytes 1048576 | tf_op jit(solution)/shard_map/all_to_all | solution.py:17
  102.0 47.7 %all-reduce.2.cloned.1.call-done = bf16[360448]{0:T(1024)(128)(2,1)} async-done(((bf16[360448]{0:T(1024)(128)(2,1)}), bf16[360448]{0:T(1024)(128)(2,1)}) %all-reduce.2.cloned.1.call-update) | async-done | bytes 720912 | tf_op jit(solution)/shard_map/psum | solution.py:44
  149.8 1.2 slice_convert_fusion.1
  150.9 1.7 reshape.401
  152.7 1.7 reshape.402
  154.4 1.1 reduce_sum.102
  155.5 0.6 reshape.388
  156.1 9.8 %all-to-all-start.3 = ((bf16[32,4,256]{2,1,0:T(4,128)(2,1)}), bf16[32,4,256]{2,1,0:T(4,128)(2,1)S(1)}, u32[]{:S(2)}, u32[]{:S(2)}) async-start(bf16[32,4,256]{2,1,0:T(4,128)(2,1)} %reshape.388), calls=%async_computation.3 | async-start | bytes 131072 | tf_op jit(solution)/shard_map/all_to_all | solution.py:124
  166.0 2.8 %convolution_convert_fusion.3 = bf16[1024,256]{1,0:T(8,128)(2,1)} fusion(bf16[176,256]{1,0:T(8,128)(2,1)S(1)} %copy-done.17, f32[1024,176]{1,0:T(8,128)} %reshape.402, f32[1024,176]{1,0:T(8,128)} %reshape.401), kind=kOutput, calls=%fused_computation.13 | convolution fusion | flops 93618176 | bytes 2056192 | tf_op jit(solution)/shard_map/dot_general | solution.py:210
  168.8 7.4 %all-to-all-done.3 = bf16[32,4,256]{2,1,0:T(4,128)(2,1)S(1)} async-done(((bf16[32,4,256]{2,1,0:T(4,128)(2,1)}), bf16[32,4,256]{2,1,0:T(4,128)(2,1)S(1)}, u32[]{:S(2)}, u32[]{:S(2)}) %all-to-all-start.3) | async-done | bytes 65568 | tf_op jit(solution)/shard_map/all_to_all | solution.py:124
  176.2 3.9 %all-to-all-start.5 = ((bf16[32,32,256]{2,1,0:T(8,128)(2,1)}), bf16[32,32,256]{2,1,0:T(8,128)(2,1)S(1)}, u32[]{:S(2)}, u32[]{:S(2)}) async-start(bf16[32,32,256]{2,1,0:T(8,128)(2,1)} %bitcast.18), calls=%async_computation.5 | async-start | bytes 1048576 | tf_op jit(solution)/shard_map/all_to_all | solution.py:17
  180.2 0.1 copy.39
  180.4 2.9 %multiply_add_fusion = f32[32,1,128,128]{3,2,1,0:T(8,128)} fusion(f32[32,1,128,128]{3,2,1,0:T(8,128)} %param.28, f32[32,128]{1,0:T(8,128)S(1)} %copy-done.9, f32[32,128]{1,0:T(8,128)S(1)} %maximum_multiply_fusion.1, f32[]{:T(128)S(6)} %sub.37), kind=kLoop, calls=%fused_computation.11 | loop fusion | flops 1572864 | bytes 4227076 | tf_op jit(solution)/shard_map/add | solution.py:83
  183.3 0.1 fusion.24
  183.5 0.7 gather_fusion
  184.2 0.1 multiply_reduce_fusion.1
  184.4 13.4 %all-to-all-done.5 = bf16[32,32,256]{2,1,0:T(8,128)(2,1)S(1)} async-done(((bf16[32,32,256]{2,1,0:T(8,128)(2,1)}), bf16[32,32,256]{2,1,0:T(8,128)(2,1)S(1)}, u32[]{:S(2)}, u32[]{:S(2)}) %all-to-all-start.5) | async-done | bytes 524320 | tf_op jit(solution)/shard_map/all_to_all | solution.py:17
  197.9 1.4 add_convert_fusion
  (54 shorter events, 0.5 us)
Async XLA Ops:
  7.2 85.5 %copy-start = (bf16[1,512,2048]{2,1,0:T(8,128)(2,1)S(1)}, bf16[1,512,2048]{2,1,0:T(8,128)(2,1)}, u32[]{:S(2)}) copy-start(bf16[1,512,2048]{2,1,0:T(8,128)(2,1)} %param.39) | copy-start | bytes 6291460
  7.2 8.4 %copy-start.1 = (bf16[32,2048]{1,0:T(8,128)(2,1)S(1)}, bf16[32,2048]{1,0:T(8,128)(2,1)}, u32[]{:S(2)}) copy-start(bf16[32,2048]{1,0:T(8,128)(2,1)} %param.20) | copy-start | bytes 393220
  7.2 8.4 %copy-start.5 = (bf16[2048,128]{1,0:T(8,128)(2,1)S(1)}, bf16[2048,128]{1,0:T(8,128)(2,1)}, u32[]{:S(2)}) copy-start(bf16[2048,128]{1,0:T(8,128)(2,1)} %param.24) | copy-start | bytes 1572868
  10.5 6.3 %copy-start.6 = (bf16[128,2048]{1,0:T(8,128)(2,1)S(1)}, bf16[128,2048]{1,0:T(8,128)(2,1)}, u32[]{:S(2)}) copy-start(bf16[128,2048]{1,0:T(8,128)(2,1)} %param.27) | copy-start | bytes 1572868
  13.4 4.9 %copy-start.7 = (f32[32,1,64]{2,0,1:T(8,128)}, f32[32,1,64]{2,0,1:T(8,128)S(1)}, u32[]{:S(2)}) copy-start(f32[32,1,64]{2,0,1:T(8,128)S(1)} %get-tuple-element.15) | copy-start | bytes 24580
  16.8 8.1 %copy-start.10 = (bf16[2048]{0:T(1024)(128)(2,1)S(1)}, bf16[2048]{0:T(1024)(128)(2,1)}, u32[]{:S(2)}) copy-start(bf16[2048]{0:T(1024)(128)(2,1)} %param.30) | copy-start | bytes 12292
  16.8 8.1 %copy-start.12 = (s32[32,2]{0,1:T(2,128)S(1)}, s32[32,2]{0,1:T(2,128)}, u32[]{:S(2)}) copy-start(s32[32,2]{0,1:T(2,128)} %param.35) | copy-start | bytes 772
  19.5 19.3 %all-to-all-start = ((bf16[8,32,2048]{2,1,0:T(8,128)(2,1)}), bf16[8,32,2048]{2,1,0:T(8,128)(2,1)S(1)}, u32[]{:S(2)}, u32[]{:S(2)}) async-start(bf16[8,32,2048]{2,1,0:T(8,128)(2,1)} %broadcast_in_dim.6), calls=%async_computation | async-start | bytes 2097152 | tf_op jit(solution)/shard_map/all_to_all | solution.py:23
  39.0 0.7 copy-start.2
  39.9 13.4 %copy-start.3 = (bf16[32,2048]{1,0:T(8,128)(2,1)}, bf16[32,2048]{1,0:T(8,128)(2,1)S(1)}, u32[]{:S(2)}) copy-start(bf16[32,2048]{1,0:T(8,128)(2,1)S(1)} %multiply_convert_fusion.2) | copy-start | bytes 393220
  40.7 28.1 %all-to-all-start.4 = ((bf16[32,32,256]{2,1,0:T(8,128)(2,1)}), bf16[32,32,256]{2,1,0:T(8,128)(2,1)S(1)}, u32[]{:S(2)}, u32[]{:S(2)}) async-start(bf16[32,32,256]{2,1,0:T(8,128)(2,1)} %broadcast_in_dim.8), calls=%async_computation.4 | async-start | bytes 1048576 | tf_op jit(solution)/shard_map/all_to_all | solution.py:23
  52.6 0.5 copy-start.13
  68.8 21.7 %all-to-all-start.1 = ((bf16[32,4,2048]{2,1,0:T(4,128)(2,1)}), bf16[32,4,2048]{2,1,0:T(4,128)(2,1)S(1)}, u32[]{:S(2)}, u32[]{:S(2)}) async-start(bf16[32,4,2048]{2,1,0:T(4,128)(2,1)} %reshape.385), calls=%async_computation.1 | async-start | bytes 1048576 | tf_op jit(solution)/shard_map/all_to_all | solution.py:116
  73.5 76.3 %all-reduce.2.cloned.1.call-start = ((), (), s32[]{:S(2)}) async-start(), calls=%async_computation.6 | async-start | bytes 1441792 | tf_op jit(solution)/shard_map/psum | solution.py:44
  95.9 58.4 %all-to-all-start.2 = ((bf16[8,128,256]{2,1,0:T(8,128)(2,1)}), bf16[8,128,256]{2,1,0:T(8,128)(2,1)}, u32[]{:S(2)}, u32[]{:S(2)}) async-start(bf16[8,128,256]{2,1,0:T(8,128)(2,1)} %bitcast.85), calls=%async_computation.2 | async-start | bytes 1048576 | tf_op jit(solution)/shard_map/all_to_all | solution.py:17
  152.7 13.3 %copy-start.17 = (bf16[176,256]{1,0:T(8,128)(2,1)S(1)}, bf16[176,256]{1,0:T(8,128)(2,1)}, u32[]{:S(2)}) copy-start(bf16[176,256]{1,0:T(8,128)(2,1)} %param.34) | copy-start | bytes 270340
  156.1 20.1 %all-to-all-start.3 = ((bf16[32,4,256]{2,1,0:T(4,128)(2,1)}), bf16[32,4,256]{2,1,0:T(4,128)(2,1)S(1)}, u32[]{:S(2)}, u32[]{:S(2)}) async-start(bf16[32,4,256]{2,1,0:T(4,128)(2,1)} %reshape.388), calls=%async_computation.3 | async-start | bytes 131072 | tf_op jit(solution)/shard_map/all_to_all | solution.py:124
  166.0 14.1 %copy-start.14 = (s32[64]{0:T(128)S(1)}, s32[64]{0:T(128)}, u32[]{:S(2)}) copy-start(s32[64]{0:T(128)} %copy-done.13) | copy-start | bytes 772
  166.0 14.1 %copy-start.16 = (s32[64,1]{0,1:T(1,128)S(1)}, s32[64,1]{0,1:T(1,128)}, u32[]{:S(2)}) copy-start(s32[64,1]{0,1:T(1,128)} %mul.310) | copy-start | bytes 772
  166.0 14.1 %copy-start.11 = (bf16[2048]{0:T(1024)(128)(2,1)S(1)}, bf16[2048]{0:T(1024)(128)(2,1)}, u32[]{:S(2)}) copy-start(bf16[2048]{0:T(1024)(128)(2,1)} %param.31) | copy-start | bytes 12292
  166.0 14.2 %copy-start.15 = (bf16[32,2]{0,1:T(2,128)(2,1)S(1)}, bf16[32,2]{0,1:T(2,128)(2,1)}, u32[]{:S(2)}) copy-start(bf16[32,2]{0,1:T(2,128)(2,1)} %param.36) | copy-start | bytes 388
  166.0 14.3 %copy-start.8 = (f32[32,1,64]{2,0,1:T(8,128)S(1)}, f32[32,1,64]{2,0,1:T(8,128)}, u32[]{:S(2)}) copy-start(f32[32,1,64]{2,0,1:T(8,128)} %copy-done.7) | copy-start | bytes 24580
  166.0 14.3 %copy-start.9 = (f32[32,128]{1,0:T(8,128)S(1)}, f32[32,128]{1,0:T(8,128)}, u32[]{:S(2)}) copy-start(f32[32,128]{1,0:T(8,128)} %get-tuple-element.16) | copy-start | bytes 49156
  176.2 21.6 %all-to-all-start.5 = ((bf16[32,32,256]{2,1,0:T(8,128)(2,1)}), bf16[32,32,256]{2,1,0:T(8,128)(2,1)S(1)}, u32[]{:S(2)}, u32[]{:S(2)}) async-start(bf16[32,32,256]{2,1,0:T(8,128)(2,1)} %bitcast.18), calls=%async_computation.5 | async-start | bytes 1048576 | tf_op jit(solution)/shard_map/all_to_all | solution.py:17
  180.4 2.9 %copy-start.4 = (bf16[32,2048]{1,0:T(8,128)(2,1)S(1)}, bf16[32,2048]{1,0:T(8,128)(2,1)}, u32[]{:S(2)}) copy-start(bf16[32,2048]{1,0:T(8,128)(2,1)} %copy-done.3) | copy-start | bytes 393220
Sparse Core Ops, SparseCore 0:
  82.2 67.4 all-reduce.1
where the time goes:
time: 207 us; the launch traced here: 206 us
  waiting for transfers between devices  105 us (51%)
  starting transfers between devices  40.5 us (20%)
  matrix products  18.1 us (9%)
  local copies, waits for them, and re-layouts  14.9 us (7%)
  between operations  14.5 us (7%)
  other arithmetic  13.4 us (6%)
    psum x1, waiting for transfers between devices, packed_total(): running = lax.psum(flat, axis)  47.7 us
    all_to_all x2, waiting for transfers between devices, copy_for_each(): return lax.all_to_all(copies, axis, split_axis=0, concat_axis=0, tiled=True)  27.9 us
    all_to_all x2, starting transfers between devices, copy_for_each(): return lax.all_to_all(copies, axis, split_axis=0, concat_axis=0, tiled=True)  16 us
    all_to_all x2, waiting for transfers between devices, sent_and_summed(): lax.all_to_all(tiles, axis, split_axis=0, concat_axis=0, tiled=True)  13.4 us
    all_to_all x2, starting transfers between devices, sent_and_summed(): lax.all_to_all(tiles, axis, split_axis=0, concat_axis=0, tiled=True)  9.98 us
    all_to_all x1, starting transfers between devices, padded_experts(): lax.all_to_all(summed.reshape(sources, items, summed.shape[1]), 'ep', spl...  9.82 us
    all_to_all x1, waiting for transfers between devices, padded_experts(): lax.all_to_all(outgoing, 'ep', split_axis=0, concat_axis=0, tiled=True)  8.34 us
    all_to_all x1, waiting for transfers between devices, padded_experts(): lax.all_to_all(summed.reshape(sources, items, summed.shape[1]), 'ep', spl...  7.39 us
  transfers between devices with their start and end apart: 7, of which 6 were waited for; matrix products, arithmetic and copies ran while one was open for 14% of the time, Pallas kernels for 0%

commit v1 on v0

v1 whole, which is shorter than its diff:
```python
import numpy as np
import jax
import jax.numpy as jnp
from jax import lax
from jax.experimental import pallas as pl
from jax.experimental.pallas import tpu as pltpu
from jax.sharding import PartitionSpec as P

EPSILON = 1e-06
THETA = 10000.0
BF = jnp.bfloat16
F32 = jnp.float32
NZ, NX, NT = 8, 4, 8


def iota(shape, dim):
    return lax.broadcasted_iota(jnp.int32, shape, dim)


def onehot(condition):
    return jnp.where(condition, 1.0, 0.0).astype(BF)


def dot(a, b):
    return jnp.dot(a, b, preferred_element_type=F32)


def as_column(row, n):
    return jnp.sum(jnp.where(iota((n, n), 0) == iota((n, n), 1), row, 0.0), axis=1, keepdims=True)


def as_row(column, n):
    return jnp.sum(jnp.where(iota((n, n), 0) == iota((n, n), 1), column, 0.0), axis=0, keepdims=True)


def step_kernel(
    resid_h, norm_gain_h, wq_h, wk_h, wv_h, wg_h, head_gain_h, wo_h, state_h, positions_h,
    ffn_gain_h, w_mix_h, dgate_h, dup_h, ddown_h, routes_h, rweight_h, eg_h, eu_h, ed_h, inv_h,
    final_h, new_state_h,
    resid, norm_gain, wqkvg, head_gain, wo, state, positions, ffn_gain, w_mix, dgate, dup, ddown,
    routes, rweight, eg, eu, ed, inv,
    mix, rs_send, rs_recv, p2_send, p2_recv, rows_x, gu, dn, part_y, yx_recv, yz_send, yz_recv,
    md_send, mz_recv, mx_send, mx_recv, ag_recv, er_send, er_recv, rx_send, rx_recv,
    rz_send, rz_recv, d5_send, d5_recv, acc, final_v,
    load_sem, out_sem,
    rs_s, rs_r, p2_s, p2_r, xz_s, xz_r, xx_s, xx_r, gw_s, gw_r, dw_s, dw_r, yx_s, yx_r, yz_s, yz_r,
    mz_s, mz_r, mx_s, mx_r, ag_s, ag_r, er_s, er_r, rx_s, rx_r, rz_s, rz_r, d5_s, d5_r,
):
    ep = lax.axis_index("ep")
    t = lax.axis_index("tp")
    z = ep // NX
    x = lax.rem(ep, NX)
    y = t // 2
    core = lax.rem(t, 2)

    def zdev(p):
        return (p * NX + x, t)

    def xdev(p):
        return (z * NX + p, t)

    def tdev(p):
        return (ep, p)

    barrier = pltpu.get_barrier_semaphore()
    for dev, me, n in ((zdev, z, NZ), (xdev, x, NX), (tdev, t, NT)):
        def greet(k, c, dev=dev, me=me, n=n):
            pl.semaphore_signal(barrier, inc=1, device_id=dev(lax.rem(me + k, n)), device_id_type=pl.DeviceIdType.MESH)
            return c
        lax.fori_loop(1, n, greet, 0)

    loads = {}
    pairs = [
        ("resid", resid_h, resid), ("norm_gain", norm_gain_h, norm_gain),
        ("wq", wq_h, wqkvg.at[:, 0:128]), ("wk", wk_h, wqkvg.at[:, 128:256]),
        ("wv", wv_h, wqkvg.at[:, 256:384]), ("wg", wg_h, wqkvg.at[:, 384:512]),
        ("positions", positions_h, positions), ("inv", inv_h, inv), ("head_gain", head_gain_h, head_gain),
        ("state", state_h.at[:, 0], state), ("wo", wo_h, wo),
        ("ffn_gain", ffn_gain_h, ffn_gain), ("w_mix", w_mix_h, w_mix),
        ("routes", routes_h, routes), ("rweight", rweight_h, rweight),
        ("dgate", dgate_h, dgate), ("dup", dup_h, dup), ("ddown", ddown_h, ddown),
        ("eg", eg_h.at[0], eg), ("eu", eu_h.at[0], eu), ("ed", ed_h.at[0], ed),
    ]
    for n, (name, src, dst) in enumerate(pairs):
        loads[name] = pltpu.make_async_copy(src, dst, load_sem.at[n])
        loads[name].start()

    def need(*names):
        for name in names:
            loads[name].wait()

    def remote(src, dst, ssem, rsem, dev):
        return pltpu.make_async_remote_copy(
            src_ref=src, dst_ref=dst, send_sem=ssem, recv_sem=rsem, device_id=dev,
            device_id_type=pl.DeviceIdType.MESH,
        )

    def send_all(n, me, dev, src_at, dst_here, ssem, rsem):
        def one(k, c):
            p = lax.rem(me + k, n)
            remote(src_at(p), dst_here, ssem.at[p], rsem.at[me], dev(p)).start()
            return c
        lax.fori_loop(1, n, one, 0)

    def recv_all(n, me, dev, src, dst_at, ssem, rsem):
        def one(k, c):
            p = lax.rem(me + k, n)
            remote(src, dst_at(p), ssem.at[p], rsem.at[p], dev(p)).wait_recv()
            return c
        lax.fori_loop(1, n, one, 0)

    def sent_all(n, me, dev, src_at, dst, ssem, rsem):
        def one(k, c):
            p = lax.rem(me + k, n)
            remote(src_at(p), dst, ssem.at[p], rsem.at[me], dev(p)).wait_send()
            return c
        lax.fori_loop(1, n, one, 0)

    need("resid", "norm_gain")
    res = resid[...].astype(F32)
    ms = jnp.mean(res * res, axis=-1, keepdims=True)
    gain_in = norm_gain[...].reshape(1, 2048).astype(F32)
    normed_in = (res * lax.rsqrt(ms + EPSILON) * gain_in).astype(BF)
    need("positions", "inv", "wq", "wk", "wv", "wg")
    angles = as_column(positions[...].astype(F32).reshape(1, 32), 32) * inv[...]
    cosine, sine = jnp.cos(angles), jnp.sin(angles)
    cos2 = jnp.concatenate([cosine, cosine], axis=-1)
    sin2 = jnp.concatenate([-sine, sine], axis=-1)
    qkvg = dot(normed_in, wqkvg[...]).astype(BF).astype(F32)

    def rotate(v):
        return v * cos2 + pltpu.roll(v, 64, 1) * sin2

    query = rotate(qkvg[:, 0:128])
    key = rotate(qkvg[:, 128:256]) * (128 ** -0.5)
    value = qkvg[:, 256:384]
    gating = qkvg[:, 384:512]
    decay = 1.0 - jnp.exp2(-1.0 - 1.5 * jnp.full((1, 128), t, jnp.int32).astype(F32))
    within = jnp.sum(query * key, axis=-1, keepdims=True) * value
    query_t = jnp.transpose(query)
    need("state")
    for s in range(32):
        mix[s : s + 1, :] = jnp.sum(state[s] * query_t[:, s : s + 1], axis=0, keepdims=True)
    need("head_gain", "wo")
    mixture = within + mix[...] * decay
    centre = jnp.mean(mixture, axis=-1, keepdims=True)
    spread = jnp.mean(jnp.square(mixture - centre), axis=-1, keepdims=True)
    normed = (mixture - centre) * lax.rsqrt(spread + EPSILON)
    normed = normed * head_gain[...].reshape(1, 128).astype(F32)
    retained = (jax.nn.silu(gating) * normed).astype(BF)
    partial = dot(retained, wo[...]).astype(BF)
    for p in range(NT):
        rs_send[p] = partial[:, 256 * p : 256 * (p + 1)]

    pl.semaphore_wait(barrier, NZ + NX + NT - 3)

    send_all(NT, t, tdev, lambda p: rs_send.at[p], rs_recv.at[t], rs_s, rs_r)
    rs_recv[t] = rs_send[t]

    key_t = jnp.transpose(key)
    for s in range(32):
        state[s] = state[s] * decay + key_t[:, s : s + 1] * value[s : s + 1, :]

    need("routes", "rweight", "dgate", "dup", "ddown", "ffn_gain", "w_mix")
    first, second = routes[:, 0:1], routes[:, 1:2]
    lane_e = iota((32, 32), 1)
    hit0, hit1 = (lane_e == first), (lane_e == second)
    both = jnp.where(hit0, 1.0, 0.0) + jnp.where(hit1, 1.0, 0.0)
    earlier = onehot(iota((32, 32), 1) < iota((32, 32), 0))
    rank = dot(earlier, both.astype(BF))
    rw = rweight[...].astype(F32)
    weight_e = jnp.where(hit0, rw[:, 0:1], 0.0) + jnp.where(hit1, rw[:, 1:2], 0.0)
    widen = onehot((iota((32, 128), 1) >> 2) == iota((32, 128), 0))
    slot = (iota((32, 128), 1) & 3).astype(F32)
    taken = dot(both.astype(BF), widen) * jnp.where(dot(rank.astype(BF), widen) == slot, 1.0, 0.0)
    combine = (dot(weight_e.astype(BF), widen) * taken).astype(BF)
    dispatch = jnp.transpose(taken).astype(BF)

    place_gate = onehot(iota((176, 384), 1) == iota((176, 384), 0))
    place_up = onehot(iota((176, 384), 1) == iota((176, 384), 0) + 176)
    gu[t] = (dot(dgate[...], place_gate) + dot(dup[...], place_up)).astype(BF)
    for p in range(NT):
        dn[p, 176:256, :] = jnp.zeros((80, 256), BF)
    dn[t, 0:176, :] = ddown[...]

    recv_all(NT, t, tdev, rs_send.at[0], lambda p: rs_recv.at[p], rs_s, rs_r)
    columns = pl.ds(pl.multiple_of(t * 256, 256), 256)
    attention = rs_recv[0].astype(F32)
    for p in range(1, NT):
        attention = attention + rs_recv[p].astype(F32)
    middle = resid[:, columns].astype(F32) + attention
    squares = as_row(jnp.sum(middle * middle, axis=-1, keepdims=True), 32)
    squares = jnp.concatenate([squares, jnp.zeros((1, 224), F32)], axis=1)

    for p in range(NT):
        p2_send[p, 0:4, :] = middle[4 * p : 4 * p + 4, :]
        p2_send[p, 4:5, :] = squares
    send_all(NT, t, tdev, lambda p: p2_send.at[p], p2_recv.at[t], p2_s, p2_r)
    p2_recv[t] = p2_send[t]
    new_state_copy = pltpu.make_async_copy(state, new_state_h.at[:, 0], out_sem.at[0])
    new_state_copy.start()
    recv_all(NT, t, tdev, p2_send.at[0], lambda p: p2_recv.at[p], p2_s, p2_r)

    total = p2_recv[0, 4:5, 0:128]
    for p in range(1, NT):
        total = total + p2_recv[p, 4:5, 0:128]
    scale = lax.rsqrt(as_column(total[:, 0:32], 32) * (1.0 / 2048) + EPSILON)
    gain_mid = ffn_gain[...].reshape(1, 2048).astype(F32)
    gain_here = gain_mid[:, 0:256]
    for p in range(1, NT):
        gain_here = jnp.where(t == p, gain_mid[:, 256 * p : 256 * (p + 1)], gain_here)
    normed_mid = (middle * scale * gain_here).astype(BF)

    outgoing = dot(dispatch, normed_mid).astype(BF)
    for p in range(NZ):
        md_send[p] = outgoing[16 * p : 16 * (p + 1), :]
    send_all(NZ, z, zdev, lambda p: md_send.at[p], mz_recv.at[z], mz_s, mz_r)
    mz_recv[z] = md_send[z]

    quarters = [
        jnp.concatenate([p2_recv[2 * q, 0:4, :], p2_recv[2 * q + 1, 0:4, :]], axis=1) for q in range(4)
    ]
    sq4 = sum(jnp.sum(v * v, axis=-1, keepdims=True) for v in quarters)
    scale4 = lax.rsqrt(sq4 * (1.0 / 2048) + EPSILON)
    mixer = w_mix[...].reshape(1, 2048).astype(F32)
    rows = [
        (quarters[q] * scale4 * gain_mid[:, 512 * q : 512 * (q + 1)]).astype(BF).astype(F32) for q in range(4)
    ]
    mixing = jax.nn.sigmoid(
        sum(jnp.sum(rows[q] * mixer[:, 512 * q : 512 * (q + 1)], axis=-1, keepdims=True) for q in range(4))
    )
    mixing16 = jnp.concatenate([mixing] * 4, axis=0)
    rows_x[x, z] = jnp.concatenate(rows, axis=0).astype(BF)
    send_all(NZ, z, zdev, lambda p: rows_x.at[x, z], rows_x.at[x, z], xz_s, xz_r)

    def to_x(zz):
        send_all(NX, x, xdev, lambda p: rows_x.at[x, zz], rows_x.at[x, zz], xx_s.at[zz], xx_r.at[zz])

    to_x(z)

    def ydev(p):
        return (ep, 2 * p + core)

    send_all(4, y, ydev, lambda p: gu.at[t], gu.at[t], gw_s, gw_r)
    send_all(4, y, ydev, lambda p: dn.at[t], dn.at[t], dw_s, dw_r)
    sibling = (ep, t + 1 - 2 * core)
    remote(gu.at[t], gu.at[t], gw_s.at[4 + y], gw_r.at[4 + y], sibling).start()
    remote(dn.at[t], dn.at[t], dw_s.at[4 + y], dw_r.at[4 + y], sibling).start()

    swap = onehot(
        iota((128, 128), 1)
        == ((iota((128, 128), 0) >> 2) & 7) * 16 + (iota((128, 128), 0) >> 5) * 4 + (iota((128, 128), 0) & 3)
    )
    unswap = onehot(
        iota((128, 128), 1)
        == ((iota((128, 128), 0) >> 2) & 3) * 32 + (iota((128, 128), 0) >> 4) * 4 + (iota((128, 128), 0) & 3)
    )
    recv_all(NZ, z, zdev, md_send.at[0], lambda p: mz_recv.at[p], mz_s, mz_r)
    swapped = dot(swap, jnp.concatenate([mz_recv[p] for p in range(NZ)], axis=0)).astype(BF)
    for p in range(NX):
        mx_send[p] = swapped[32 * p : 32 * (p + 1), :]
    send_all(NX, x, xdev, lambda p: mx_send.at[p], mx_recv.at[x], mx_s, mx_r)
    mx_recv[x] = mx_send[x]

    def pass_on(k, c):
        p = lax.rem(z + k, NZ)
        remote(rows_x.at[x, p], rows_x.at[x, p], xz_s.at[p], xz_r.at[p], zdev(p)).wait_recv()
        to_x(p)
        return c
    lax.fori_loop(1, NZ, pass_on, 0)

    recv_all(NX, x, xdev, mx_send.at[0], lambda p: mx_recv.at[p], mx_s, mx_r)
    ag_recv[t] = jnp.concatenate([mx_recv[p] for p in range(NX)], axis=0)
    send_all(NT, t, tdev, lambda p: ag_recv.at[t], ag_recv.at[t], ag_s, ag_r)

    def hand_over(k, c):
        p = lax.rem(y + k, 4)
        tt = 2 * p + core
        remote(gu.at[tt], gu.at[tt], gw_s.at[p], gw_r.at[p], ydev(p)).wait_recv()
        remote(gu.at[tt], gu.at[tt], gw_s.at[4 + p], gw_r.at[4 + p], sibling).start()
        remote(dn.at[tt], dn.at[tt], dw_s.at[p], dw_r.at[p], ydev(p)).wait_recv()
        remote(dn.at[tt], dn.at[tt], dw_s.at[4 + p], dw_r.at[4 + p], sibling).start()
        return c
    lax.fori_loop(1, 4, hand_over, 0)

    def all_weights(k, c):
        tt = 2 * k + 1 - core
        remote(gu.at[tt], gu.at[tt], gw_s.at[4 + k], gw_r.at[4 + k], sibling).wait_recv()
        remote(dn.at[tt], dn.at[tt], dw_s.at[4 + k], dw_r.at[4 + k], sibling).wait_recv()
        return c
    lax.fori_loop(0, 4, all_weights, 0)

    def rows_in(zz, c):
        recv_all(NX, x, xdev, rows_x.at[x, zz], lambda p: rows_x.at[p, zz], xx_s.at[zz], xx_r.at[zz])
        return c
    lax.fori_loop(0, NZ, rows_in, 0)

    tiles = rows_x[...].reshape(512, 512)
    spread_row = iota((128, 512), 0)
    spread_col = iota((128, 512), 1)
    gate_up = jnp.zeros((128, 384), F32)
    for q in range(4):
        take = onehot(spread_col == (spread_row >> 2) * 16 + 4 * q + (spread_row & 3))
        block = dot(take, tiles).astype(BF)
        gate_up = gate_up + dot(block, gu[2 * q : 2 * q + 2].reshape(512, 384))
    up = pltpu.roll(gate_up, 384 - 176, 1)
    hidden = jnp.where(iota((128, 256), 1) < 176, jax.nn.silu(gate_up[:, 0:256]) * up[:, 0:256], 0.0).astype(BF)
    back_row = iota((512, 128), 0)
    back_col = iota((512, 128), 1)
    packed = jnp.zeros((512, 512), F32)
    for q in range(4):
        block = jnp.concatenate([dot(hidden, dn[2 * q]), dot(hidden, dn[2 * q + 1])], axis=1).astype(BF)
        put = onehot(back_row == (back_col >> 2) * 16 + 4 * q + (back_col & 3))
        packed = packed + dot(put, block)
    part_y[...] = packed.astype(BF).reshape(NX, 128, 512)
    send_all(NX, x, xdev, lambda p: part_y.at[p], yx_recv.at[x], yx_s, yx_r)
    yx_recv[x] = part_y[x]

    need("eg", "eu", "ed")

    def chunk(p, c):
        @pl.when(p != t)
        def _():
            remote(ag_recv.at[t], ag_recv.at[p], ag_s.at[p], ag_r.at[p], tdev(p)).wait_recv()
        depth = pl.ds(pl.multiple_of(p * 256, 256), 256)
        rows_p = ag_recv[p]
        acc[:, 0:512] += dot(rows_p, eg[depth, :])
        acc[:, 512:1024] += dot(rows_p, eu[depth, :])
        return c
    acc[...] = jnp.zeros_like(acc)
    lax.fori_loop(0, NT, chunk, 0)
    hidden_e = (jax.nn.silu(acc[:, 0:512]) * acc[:, 512:1024]).astype(BF)

    def down(k, c):
        p = lax.rem(t + 1 + k, NT)
        er_send[p] = dot(hidden_e, ed[:, pl.ds(pl.multiple_of(p * 256, 256), 256)]).astype(BF)
        @pl.when(p != t)
        def _():
            remote(er_send.at[p], er_recv.at[t], er_s.at[p], er_r.at[t], tdev(p)).start()
        return c
    lax.fori_loop(0, NT, down, 0)
    er_recv[t] = er_send[t]

    recv_all(NX, x, xdev, part_y.at[0], lambda p: yx_recv.at[p], yx_s, yx_r)
    summed = yx_recv[0].astype(F32)
    for p in range(1, NX):
        summed = summed + yx_recv[p].astype(F32)
    yz_send[...] = summed.astype(BF).reshape(NZ, 16, 512)
    send_all(NZ, z, zdev, lambda p: yz_send.at[p], yz_recv.at[z], yz_s, yz_r)
    yz_recv[z] = yz_send[z]

    recv_all(NT, t, tdev, er_send.at[0], lambda p: er_recv.at[p], er_s, er_r)
    result = er_recv[0].astype(F32)
    for p in range(1, NT):
        result = result + er_recv[p].astype(F32)
    rx_send[...] = result.astype(BF).reshape(NX, 32, 256)
    send_all(NX, x, xdev, lambda p: rx_send.at[p], rx_recv.at[x], rx_s, rx_r)
    rx_recv[x] = rx_send[x]

    recv_all(NZ, z, zdev, yz_send.at[0], lambda p: yz_recv.at[p], yz_s, yz_r)
    dense = yz_recv[0].astype(F32)
    for p in range(1, NZ):
        dense = dense + yz_recv[p].astype(F32)
    dense = dense * mixing16
    for p in range(NT):
        q, half = p // 2, p % 2
        d5_send[p, 0:4, :] = dense[4 * q : 4 * q + 4, 256 * half : 256 * (half + 1)]
        d5_send[p, 4:8, :] = jnp.zeros((4, 256), F32)
    send_all(NT, t, tdev, lambda p: d5_send.at[p], d5_recv.at[t], d5_s, d5_r)
    d5_recv[t] = d5_send[t]

    recv_all(NX, x, xdev, rx_send.at[0], lambda p: rx_recv.at[p], rx_s, rx_r)
    home = dot(unswap, jnp.concatenate([rx_recv[p] for p in range(NX)], axis=0)).astype(BF)
    for p in range(NZ):
        rz_send[p] = home[16 * p : 16 * (p + 1), :]
    send_all(NZ, z, zdev, lambda p: rz_send.at[p], rz_recv.at[z], rz_s, rz_r)
    rz_recv[z] = rz_send[z]

    recv_all(NT, t, tdev, d5_send.at[0], lambda p: d5_recv.at[p], d5_s, d5_r)
    dense_rows = jnp.concatenate([d5_recv[p, 0:4, :] for p in range(NT)], axis=0)
    recv_all(NZ, z, zdev, rz_send.at[0], lambda p: rz_recv.at[p], rz_s, rz_r)
    moe = dot(combine, jnp.concatenate([rz_recv[p] for p in range(NZ)], axis=0))
    final_v[...] = (middle + moe + dense_rows).astype(BF)
    final_copy = pltpu.make_async_copy(final_v, final_h, out_sem.at[1])
    final_copy.start()

    sent_all(NT, t, tdev, lambda p: rs_send.at[p], rs_recv.at[t], rs_s, rs_r)
    sent_all(NT, t, tdev, lambda p: p2_send.at[p], p2_recv.at[t], p2_s, p2_r)
    sent_all(NZ, z, zdev, lambda p: md_send.at[p], mz_recv.at[z], mz_s, mz_r)
    sent_all(NZ, z, zdev, lambda p: rows_x.at[x, z], rows_x.at[x, z], xz_s, xz_r)

    def x_sent(zz, c):
        sent_all(NX, x, xdev, lambda p: rows_x.at[x, zz], rows_x.at[x, zz], xx_s.at[zz], xx_r.at[zz])
        return c
    lax.fori_loop(0, NZ, x_sent, 0)
    sent_all(4, y, ydev, lambda p: gu.at[t], gu.at[t], gw_s, gw_r)
    sent_all(4, y, ydev, lambda p: dn.at[t], dn.at[t], dw_s, dw_r)

    def w_sent(k, c):
        tt = 2 * k + core
        remote(gu.at[tt], gu.at[tt], gw_s.at[4 + k], gw_r.at[4 + k], sibling).wait_send()
        remote(dn.at[tt], dn.at[tt], dw_s.at[4 + k], dw_r.at[4 + k], sibling).wait_send()
        return c
    lax.fori_loop(0, 4, w_sent, 0)
    sent_all(NX, x, xdev, lambda p: mx_send.at[p], mx_recv.at[x], mx_s, mx_r)
    sent_all(NT, t, tdev, lambda p: ag_recv.at[t], ag_recv.at[t], ag_s, ag_r)
    sent_all(NX, x, xdev, lambda p: part_y.at[p], yx_recv.at[x], yx_s, yx_r)
    sent_all(NT, t, tdev, lambda p: er_send.at[p], er_recv.at[t], er_s, er_r)
    sent_all(NZ, z, zdev, lambda p: yz_send.at[p], yz_recv.at[z], yz_s, yz_r)
    sent_all(NX, x, xdev, lambda p: rx_send.at[p], rx_recv.at[x], rx_s, rx_r)
    sent_all(NT, t, tdev, lambda p: d5_send.at[p], d5_recv.at[t], d5_s, d5_r)
    sent_all(NZ, z, zdev, lambda p: rz_send.at[p], rz_recv.at[z], rz_s, rz_r)
    new_state_copy.wait()
    final_copy.wait()


def per_device(*args):
    inv = jnp.asarray((THETA ** (-np.arange(64) / 64.0)).astype(np.float32)[None, :])
    dma = pltpu.SemaphoreType.DMA
    vmem = pltpu.VMEM
    scratch = [
        vmem((32, 2048), BF), vmem((2048,), BF), vmem((2048, 512), BF), vmem((128,), BF),
        vmem((128, 2048), BF), vmem((32, 128, 128), F32), vmem((32,), jnp.int32), vmem((2048,), BF),
        vmem((2048,), BF), vmem((256, 176), BF), vmem((256, 176), BF), vmem((176, 256), BF),
        vmem((32, 2), jnp.int32), vmem((32, 2), BF), vmem((2048, 512), BF), vmem((2048, 512), BF),
        vmem((512, 2048), BF), vmem((1, 64), F32),
        vmem((32, 128), F32), vmem((8, 32, 256), BF), vmem((8, 32, 256), BF),
        vmem((8, 8, 256), F32), vmem((8, 8, 256), F32), vmem((4, 8, 16, 512), BF),
        vmem((8, 256, 384), BF), vmem((8, 256, 256), BF), vmem((4, 128, 512), BF), vmem((4, 128, 512), BF),
        vmem((8, 16, 512), BF), vmem((8, 16, 512), BF),
        vmem((8, 16, 256), BF), vmem((8, 16, 256), BF), vmem((4, 32, 256), BF), vmem((4, 32, 256), BF),
        vmem((8, 128, 256), BF), vmem((8, 128, 256), BF), vmem((8, 128, 256), BF),
        vmem((4, 32, 256), BF), vmem((4, 32, 256), BF), vmem((8, 16, 256), BF), vmem((8, 16, 256), BF),
        vmem((8, 8, 256), F32), vmem((8, 8, 256), F32), vmem((128, 1024), F32), vmem((32, 256), BF),
        dma((21,)), dma((2,)),
        dma((8,)), dma((8,)), dma((8,)), dma((8,)), dma((8,)), dma((8,)), dma((8, 4)), dma((8, 4)),
        dma((8,)), dma((8,)), dma((8,)), dma((8,)), dma((4,)), dma((4,)), dma((8,)), dma((8,)),
        dma((8,)), dma((8,)), dma((4,)), dma((4,)), dma((8,)), dma((8,)), dma((8,)), dma((8,)),
        dma((4,)), dma((4,)), dma((8,)), dma((8,)), dma((8,)), dma((8,)),
    ]
    hbm = pl.BlockSpec(memory_space=pl.ANY)
    return pl.pallas_call(
        step_kernel,
        out_shape=(
            jax.ShapeDtypeStruct((32, 256), BF),
            jax.ShapeDtypeStruct((32, 1, 128, 128), F32),
        ),
        in_specs=[hbm] * 21,
        out_specs=(hbm, hbm),
        scratch_shapes=scratch,
        compiler_params=pltpu.CompilerParams(
            collective_id=0, has_side_effects=True, vmem_limit_bytes=60 * 1024 * 1024
        ),
    )(*args, inv)


def solution(mesh):
    in_specs = (
        P("ep", None), P(), P(None, "tp"), P(None, "tp"), P(None, "tp"), P(None, "tp"), P("tp"),
        P("tp", None), P("ep", "tp", None, None), P("ep"), P(), P(), P("tp", "ep"), P("tp", "ep"),
        P("ep", "tp"), P("ep", None), P("ep", None), P("ep", None, "tp"), P("ep", None, "tp"),
        P("ep", "tp", None),
    )
    out_specs = (P("ep", "tp"), P("ep", "tp", None, None))
    return jax.shard_map(per_device, mesh=mesh, in_specs=in_specs, out_specs=out_specs, check_vma=False)
```

time: 207 us -> 74.1 us (0.36)
  the two profiles are of different devices: /device:TPU:24 before, /device:TPU:1 now
where the time goes in v1:
time: 74.1 us; the launch traced here: 73.9 us
  Pallas kernels  62.8 us (85%)
  local copies, waits for them, and re-layouts  10.5 us (14%)
    pallas_call x1, Pallas kernels, per_device(): pl.pallas_call(step_kernel, out_shape=(jax.ShapeDtypeStruct((32, 256), BF...  62.8 us
    unnamed x6, local copies, waits for them, and re-layouts  10.5 us

profile of v1, /device:TPU:1, one launch (start us, length us, event | category | flops | bytes accessed | tf_op | source)
XLA Modules:
  0.0 73.9 jit_solution(7480424936697452463)
XLA Ops:
  0.6 1.3 %copy.26.rweight_h = bf16[32,2]{1,0:T(8,128)(2,1)} copy(bf16[32,2]{0,1:T(2,128)(2,1)} %param.37) | data formatting | bytes 256 | tf_op args[16]
  2.0 1.4 %copy.25.routes_h = s32[32,2]{1,0:T(8,128)} copy(s32[32,2]{0,1:T(2,128)} %param.36) | data formatting | bytes 512 | tf_op args[15]
  3.3 1.6 %copy.23.dgate_h = bf16[256,176]{1,0:T(8,128)(2,1)} copy(bf16[256,176]{0,1:T(8,128)(2,1)} %param.33) | data formatting | bytes 180224 | tf_op args[12]
  5.0 1.7 %copy.24.dup_h = bf16[256,176]{1,0:T(8,128)(2,1)} copy(bf16[256,176]{0,1:T(8,128)(2,1)} %param.34) | data formatting | bytes 180224 | tf_op args[13]
  6.6 62.8 %shard_map.212 = (bf16[32,256]{1,0:T(8,128)(2,1)}, f32[32,1,128,128]{3,2,1,0:T(8,128)}) custom-call(bf16[32,2048]{1,0:T(8,128)(2,1)} %resid_h.1, bf16[2048]{0:T(1024)(128)(2,1)} %norm_gain_h.1, bf16[2048,128]{1,0:T(8,128)(2,1)} %wq_h.1, bf16[2048,128]{1,0:T(8,128)(2,1)} %wk_h.1, bf16[2048,128]{1,0:T(8,128)(2,1)} %wv_h.1, bf16[2048,128]{1,0:T(8,128)(2,1)} %wg_h.1, ...), custom_call_target="tpu_custom_call" | custom-call | tf_op jit(solution)/shard_map/pallas_call | solution.py:442
  69.4 1.3 %copy.29 = bf16[32,256]{1,0:T(8,128)(2,1)} copy(bf16[32,256]{1,0:T(8,128)(2,1)} %get-tuple-element.4) | data formatting | bytes 32768
  70.7 3.1 %copy.30 = f32[32,1,128,128]{3,2,1,0:T(8,128)} copy(f32[32,1,128,128]{3,2,1,0:T(8,128)} %get-tuple-element.5) | data formatting | bytes 4194304

commit v2 on v1

v2 whole, which is shorter than its diff:
```python
import numpy as np
import jax
import jax.numpy as jnp
from jax import lax
from jax.experimental import pallas as pl
from jax.experimental.pallas import tpu as pltpu
from jax.sharding import PartitionSpec as P

EPSILON = 1e-06
THETA = 10000.0
BF = jnp.bfloat16
F32 = jnp.float32
NZ, NX, NT, NE = 8, 4, 8, 32


def iota(shape, dim):
    return lax.broadcasted_iota(jnp.int32, shape, dim)


def onehot(condition):
    return jnp.where(condition, 1.0, 0.0).astype(BF)


def dot(a, b):
    return jnp.dot(a, b, preferred_element_type=F32)


def dot_nt(a, b):
    return lax.dot_general(a, b, (((1,), (1,)), ((), ())), preferred_element_type=F32)


def as_column(row, n):
    return jnp.sum(jnp.where(iota((n, n), 0) == iota((n, n), 1), row, 0.0), axis=1, keepdims=True)


def as_row(column, n):
    return jnp.sum(jnp.where(iota((n, n), 0) == iota((n, n), 1), column, 0.0), axis=0, keepdims=True)


def step_kernel(
    resid_h, norm_gain_h, wq_h, wk_h, wv_h, wg_h, head_gain_h, wo_h, state_h, positions_h,
    ffn_gain_h, w_mix_h, dgate_h, dup_h, ddown_h, routes_h, rweight_h, eg_h, eu_h, ed_h, inv_h,
    final_v, new_state,
    resid, norm_gain, wqkvg, head_gain, wo, state, positions, ffn_gain, w_mix,
    routes, rweight, eg, eu, ed, inv,
    mix, rs_send, rs_recv, p2_send, p2_recv, rows_x, dw, part_y, yx_recv, yz_send, yz_recv,
    md_send, md_recv, ag_recv, pair_send, pair_recv, er_own, er_send, er_recv, mr_send, mr_recv,
    d5_send, d5_recv, acc,
    load_sem,
    rs_s, rs_r, p2_s, p2_r, xz_s, xz_r, xx_s, xx_r, wy_s, wy_r, wc_s, wc_r, yx_s, yx_r, yz_s, yz_r,
    md_s, md_r, ag_s, ag_r, ac_s, pair_s, pair_r, er_s, er_r, mr_s, mr_r, d5_s, d5_r,
):
    ep = lax.axis_index("ep")
    t = lax.axis_index("tp")
    z = ep // NX
    x = lax.rem(ep, NX)
    y = t // 2
    core = lax.rem(t, 2)

    def zdev(p):
        return (p * NX + x, t)

    def xdev(p):
        return (z * NX + p, t)

    def tdev(p):
        return (ep, p)

    def ydev(p):
        return (ep, 2 * p + core)

    def edev(p):
        return (p, t)

    sibling = (ep, t + 1 - 2 * core)

    scope = []

    def phase(name):
        if scope:
            scope.pop().__exit__(None, None, None)
        if name:
            scope.append(jax.named_scope(name))
            scope[0].__enter__()

    phase("greet")
    barrier = pltpu.get_barrier_semaphore()
    for dev, me, n in ((edev, ep, NE), (tdev, t, NT)):
        def greet(k, c, dev=dev, me=me, n=n):
            pl.semaphore_signal(barrier, inc=1, device_id=dev(lax.rem(me + k, n)), device_id_type=pl.DeviceIdType.MESH)
            return c
        lax.fori_loop(1, n, greet, 0)

    loads = {}
    pairs = [
        ("resid", resid_h, resid), ("norm_gain", norm_gain_h, norm_gain),
        ("wq", wq_h, wqkvg.at[:, 0:128]), ("wk", wk_h, wqkvg.at[:, 128:256]),
        ("wv", wv_h, wqkvg.at[:, 256:384]), ("wg", wg_h, wqkvg.at[:, 384:512]),
        ("positions", positions_h, positions), ("inv", inv_h, inv), ("head_gain", head_gain_h, head_gain),
        ("state", state_h.at[:, 0], state), ("wo", wo_h, wo),
        ("ffn_gain", ffn_gain_h, ffn_gain), ("w_mix", w_mix_h, w_mix),
        ("routes", routes_h, routes), ("rweight", rweight_h, rweight),
        ("ddown", ddown_h, dw.at[t, 0:176]), ("dgate", dgate_h, dw.at[t, 176:352]),
        ("dup", dup_h, dw.at[t, 352:528]),
        ("eg", eg_h.at[0], eg), ("eu", eu_h.at[0], eu), ("ed", ed_h.at[0], ed),
    ]
    for n, (name, src, dst) in enumerate(pairs):
        loads[name] = pltpu.make_async_copy(src, dst, load_sem.at[n])
        loads[name].start()

    def need(*names):
        for name in names:
            loads[name].wait()

    def remote(src, dst, ssem, rsem, dev):
        return pltpu.make_async_remote_copy(
            src_ref=src, dst_ref=dst, send_sem=ssem, recv_sem=rsem, device_id=dev,
            device_id_type=pl.DeviceIdType.MESH,
        )

    def send_all(n, me, dev, src_at, dst_here, ssem, rsem):
        def one(k, c):
            p = lax.rem(me + k, n)
            remote(src_at(p), dst_here, ssem.at[p], rsem.at[me], dev(p)).start()
            return c
        lax.fori_loop(1, n, one, 0)

    def recv_all(n, me, dev, src, dst_at, ssem, rsem):
        def one(k, c):
            p = lax.rem(me + k, n)
            remote(src, dst_at(p), ssem.at[p], rsem.at[p], dev(p)).wait_recv()
            return c
        lax.fori_loop(1, n, one, 0)

    def sent_all(n, me, dev, src_at, dst, ssem, rsem):
        def one(k, c):
            p = lax.rem(me + k, n)
            remote(src_at(p), dst, ssem.at[p], rsem.at[me], dev(p)).wait_send()
            return c
        lax.fori_loop(1, n, one, 0)

    phase("retention")
    need("resid", "norm_gain")
    res = resid[...].astype(F32)
    ms = jnp.mean(res * res, axis=-1, keepdims=True)
    gain_in = norm_gain[...].reshape(1, 2048).astype(F32)
    normed_in = (res * lax.rsqrt(ms + EPSILON) * gain_in).astype(BF)
    need("positions", "inv", "wq", "wk", "wv", "wg")
    angles = as_column(positions[...].astype(F32).reshape(1, 32), 32) * inv[...]
    cosine, sine = jnp.cos(angles), jnp.sin(angles)
    cos2 = jnp.concatenate([cosine, cosine], axis=-1)
    sin2 = jnp.concatenate([-sine, sine], axis=-1)
    qkvg = dot(normed_in, wqkvg[...]).astype(BF).astype(F32)

    def rotate(v):
        return v * cos2 + pltpu.roll(v, 64, 1) * sin2

    query = rotate(qkvg[:, 0:128])
    key = rotate(qkvg[:, 128:256]) * (128 ** -0.5)
    value = qkvg[:, 256:384]
    gating = qkvg[:, 384:512]
    decay = 1.0 - jnp.exp2(-1.0 - 1.5 * jnp.full((1, 128), t, jnp.int32).astype(F32))
    within = jnp.sum(query * key, axis=-1, keepdims=True) * value
    query_t = jnp.transpose(query)
    phase("state")
    need("state")
    for s in range(32):
        mix[s : s + 1, :] = jnp.sum(state[s] * query_t[:, s : s + 1], axis=0, keepdims=True)
    phase("head_out")
    need("head_gain", "wo")
    mixture = within + mix[...] * decay
    centre = jnp.mean(mixture, axis=-1, keepdims=True)
    spread = jnp.mean(jnp.square(mixture - centre), axis=-1, keepdims=True)
    normed = (mixture - centre) * lax.rsqrt(spread + EPSILON)
    normed = normed * head_gain[...].reshape(1, 128).astype(F32)
    retained = (jax.nn.silu(gating) * normed).astype(BF)
    partial = dot(retained, wo[...]).astype(BF)
    for p in range(NT):
        rs_send[p] = partial[:, 256 * p : 256 * (p + 1)]

    phase("barrier")
    pl.semaphore_wait(barrier, NE + NT - 2)

    phase("rs_send")
    send_all(NT, t, tdev, lambda p: rs_send.at[p], rs_recv.at[t], rs_s, rs_r)
    rs_recv[t] = rs_send[t]

    need("ddown", "dgate", "dup")
    mine = dw.at[t, 0:528]
    remote(mine, mine, wc_s.at[y], wc_r.at[y], sibling).start()

    key_t = jnp.transpose(key)
    for s in range(32):
        new_state[s, 0] = state[s] * decay + key_t[:, s : s + 1] * value[s : s + 1, :]

    need("routes", "rweight", "ffn_gain", "w_mix")
    ids = jnp.transpose(routes[...].astype(F32))
    rw = jnp.transpose(rweight[...].astype(F32))
    lane_e = iota((32, 32), 1).astype(F32)
    hit0, hit1 = (lane_e == ids[:, 0:1]), (lane_e == ids[:, 1:2])
    both = jnp.where(hit0, 1.0, 0.0) + jnp.where(hit1, 1.0, 0.0)
    earlier = onehot(iota((32, 32), 1) < iota((32, 32), 0))
    rank = dot(earlier, both.astype(BF))
    weight_e = jnp.where(hit0, rw[:, 0:1], 0.0) + jnp.where(hit1, rw[:, 1:2], 0.0)
    lane = iota((32, 256), 1)
    widen = onehot((lane >> 3) == iota((32, 256), 0))
    slot = (lane & 3).astype(F32)
    taken = dot(both.astype(BF), widen) * jnp.where(dot(rank.astype(BF), widen) == slot, 1.0, 0.0)
    weighted = dot(weight_e.astype(BF), widen) * taken
    halves = [((lane >> 2) & 1) == h for h in range(2)]
    dispatch = [jnp.transpose(jnp.where(halves[h], taken, 0.0)).astype(BF) for h in range(2)]
    combine = [jnp.where(halves[h], weighted, 0.0).astype(BF) for h in range(2)]
    up_row, up_col = iota((128, 256), 0), iota((128, 256), 1)
    unpack = [onehot(up_col == (up_row >> 2) * 8 + 4 * h + (up_row & 3)) for h in range(2)]
    pk_row, pk_col = iota((256, 128), 0), iota((256, 128), 1)
    pack = [onehot(pk_row == (pk_col >> 2) * 8 + 4 * h + (pk_col & 3)) for h in range(2)]
    for p in range(NT):
        dw[p, 528:560, :] = jnp.zeros((32, 256), BF)

    phase("rs_wait")
    recv_all(NT, t, tdev, rs_send.at[0], lambda p: rs_recv.at[p], rs_s, rs_r)
    phase("middle")
    columns = pl.ds(pl.multiple_of(t * 256, 256), 256)
    attention = rs_recv[0].astype(F32)
    for p in range(1, NT):
        attention = attention + rs_recv[p].astype(F32)
    middle = resid[:, columns].astype(F32) + attention
    squares = as_row(jnp.sum(middle * middle, axis=-1, keepdims=True), 32)
    squares = jnp.concatenate([squares, jnp.zeros((1, 224), F32)], axis=1)

    for p in range(NT):
        p2_send[p, 0:4, :] = middle[4 * p : 4 * p + 4, :]
        p2_send[p, 4:5, :] = squares
    send_all(NT, t, tdev, lambda p: p2_send.at[p], p2_recv.at[t], p2_s, p2_r)
    p2_recv[t] = p2_send[t]
    ahead, behind = lax.rem(y + 1, 4), lax.rem(y + 3, 4)
    onward = lax.rem(y + 1 + 2 * core, 4)
    origin = lax.rem(y + 3 + 2 * core, 4)
    across = lax.rem(y + 2, 4)
    remote(mine, mine, wy_s.at[0], wy_r.at[y], ydev(ahead)).start()
    remote(mine, mine, wy_s.at[1], wy_r.at[y], ydev(behind)).start()
    phase("p2_wait")
    recv_all(NT, t, tdev, p2_send.at[0], lambda p: p2_recv.at[p], p2_s, p2_r)

    phase("norms")
    total = p2_recv[0, 4:5, 0:128]
    for p in range(1, NT):
        total = total + p2_recv[p, 4:5, 0:128]
    scale = lax.rsqrt(as_column(total[:, 0:32], 32) * (1.0 / 2048) + EPSILON)
    gain_mid = ffn_gain[...].reshape(1, 2048).astype(F32)
    gain_here = gain_mid[:, 0:256]
    for p in range(1, NT):
        gain_here = jnp.where(t == p, gain_mid[:, 256 * p : 256 * (p + 1)], gain_here)
    normed_mid = (middle * scale * gain_here).astype(BF)

    outgoing = dot(dispatch[0], normed_mid[:, 0:128]) + dot(dispatch[1], normed_mid[:, 128:256])
    md_send[...] = outgoing.astype(BF).reshape(NE, 8, 128)
    far = 16

    def spread_out(src_at, dst_here, ssem, rsem):
        def one(k, c):
            p = lax.rem(ep + lax.rem(k + far, NE - 1) + 1, NE)
            remote(src_at(p), dst_here, ssem.at[p], rsem.at[ep], edev(p)).start()
            return c
        lax.fori_loop(0, NE - 1, one, 0)

    spread_out(lambda p: md_send.at[p], md_recv.at[ep], md_s, md_r)
    md_recv[ep] = md_send[ep]

    quarters = [
        jnp.concatenate([p2_recv[2 * q, 0:4, :], p2_recv[2 * q + 1, 0:4, :]], axis=1) for q in range(4)
    ]
    sq4 = sum(jnp.sum(v * v, axis=-1, keepdims=True) for v in quarters)
    scale4 = lax.rsqrt(sq4 * (1.0 / 2048) + EPSILON)
    mixer = w_mix[...].reshape(1, 2048).astype(F32)
    rows = [
        (quarters[q] * scale4 * gain_mid[:, 512 * q : 512 * (q + 1)]).astype(BF).astype(F32) for q in range(4)
    ]
    mixing = jax.nn.sigmoid(
        sum(jnp.sum(rows[q] * mixer[:, 512 * q : 512 * (q + 1)], axis=-1, keepdims=True) for q in range(4))
    )
    mixing16 = jnp.concatenate([mixing] * 4, axis=0)
    rows_x[x, z] = jnp.concatenate(rows, axis=0).astype(BF)
    send_all(NZ, z, zdev, lambda p: rows_x.at[x, z], rows_x.at[x, z], xz_s, xz_r)

    def to_x(zz):
        send_all(NX, x, xdev, lambda p: rows_x.at[x, zz], rows_x.at[x, zz], xx_s.at[zz], xx_r.at[zz])

    to_x(z)

    phase("relay")

    def weights_of(p):
        return dw.at[2 * p + core, 0:528]

    def from_y(p, slot):
        return remote(weights_of(p), weights_of(p), wy_s.at[slot], wy_r.at[p], ydev(p))

    def to_sibling(p):
        return remote(weights_of(p), weights_of(p), wc_s.at[p], wc_r.at[p], sibling)

    relayed = remote(weights_of(origin), weights_of(origin), wy_s.at[2], wy_r.at[origin], ydev(onward))
    from_y(origin, 2).wait_recv()
    relayed.start()
    to_sibling(origin).start()
    from_y(onward, 2).wait_recv()
    to_sibling(onward).start()

    phase("md_wait")
    recv_all(NE, ep, edev, md_send.at[0], lambda p: md_recv.at[p], md_s, md_r)
    arrived = md_recv[...].reshape(256, 128)
    ag_recv[t] = jnp.concatenate([dot(unpack[h], arrived) for h in range(2)], axis=1).astype(BF)
    own_rows = ag_recv.at[t]

    def group_send(k, c):
        p = lax.rem(y + 4 - k, 4)
        remote(own_rows, own_rows, ag_s.at[p], ag_r.at[t], ydev(p)).start()
        return c
    lax.fori_loop(1, 4, group_send, 0)
    remote(own_rows, own_rows, ac_s.at[y], ag_r.at[t], sibling).start()

    phase("xz_wait")
    def pass_on(k, c):
        p = lax.rem(z + k, NZ)
        remote(rows_x.at[x, p], rows_x.at[x, p], xz_s.at[p], xz_r.at[p], zdev(p)).wait_recv()
        to_x(p)
        return c
    lax.fori_loop(1, NZ, pass_on, 0)

    phase("weights_wait")
    from_y(across, 2).wait_recv()
    to_sibling(across).start()

    def all_weights(k, c):
        theirs = dw.at[2 * k + 1 - core, 0:528]
        remote(theirs, theirs, wc_s.at[k], wc_r.at[k], sibling).wait_recv()
        return c
    lax.fori_loop(0, 4, all_weights, 0)

    def rows_in(zz, c):
        recv_all(NX, x, xdev, rows_x.at[x, zz], lambda p: rows_x.at[p, zz], xx_s.at[zz], xx_r.at[zz])
        return c

    phase("xx_wait")
    lax.fori_loop(0, NZ, rows_in, 0)

    phase("dense_mm")
    tiles = rows_x[...].reshape(512, 512)
    spread_row = iota((128, 512), 0)
    spread_col = iota((128, 512), 1)
    gate_up = jnp.zeros((128, 384), F32)
    for q in range(4):
        take = onehot(spread_col == (spread_row >> 2) * 16 + 4 * q + (spread_row & 3))
        block = dot(take, tiles).astype(BF)
        gate_up = gate_up + dot_nt(block[:, 0:256], dw[2 * q, 176:560])
        gate_up = gate_up + dot_nt(block[:, 256:512], dw[2 * q + 1, 176:560])
    up = pltpu.roll(gate_up, 384 - 176, 1)
    hidden = jnp.where(iota((128, 256), 1) < 176, jax.nn.silu(gate_up[:, 0:256]) * up[:, 0:256], 0.0).astype(BF)
    back_row = iota((512, 128), 0)
    back_col = iota((512, 128), 1)
    packed = jnp.zeros((512, 512), F32)
    for q in range(4):
        block = jnp.concatenate([dot(hidden, dw[2 * q, 0:256]), dot(hidden, dw[2 * q + 1, 0:256])], axis=1).astype(BF)
        put = onehot(back_row == (back_col >> 2) * 16 + 4 * q + (back_col & 3))
        packed = packed + dot(put, block)
    part_y[...] = packed.astype(BF).reshape(NX, 128, 512)
    send_all(NX, x, xdev, lambda p: part_y.at[p], yx_recv.at[x], yx_s, yx_r)
    yx_recv[x] = part_y[x]

    phase("ag_gate_up")
    need("eg", "eu", "ed")

    def chunk(p):
        depth = pl.ds(pl.multiple_of(p * 256, 256), 256)
        rows_p = ag_recv[p]
        acc[:, 0:512] += dot(rows_p, eg[depth, :])
        acc[:, 512:1024] += dot(rows_p, eu[depth, :])

    acc[...] = jnp.zeros_like(acc)

    def two_chunks(k, c):
        p = lax.rem(y + k + k // 2, 4)
        p = jnp.where(k == 3, across, p)
        direct, other = 2 * p + core, 2 * p + 1 - core

        @pl.when(k > 0)
        def _():
            remote(ag_recv.at[direct], ag_recv.at[direct], ag_s.at[p], ag_r.at[direct], ydev(p)).wait_recv()
            remote(ag_recv.at[direct], ag_recv.at[direct], ac_s.at[p], ag_r.at[direct], sibling).start()
        chunk(direct)
        remote(ag_recv.at[other], ag_recv.at[other], ac_s.at[p], ag_r.at[other], sibling).wait_recv()
        chunk(other)
        return c
    lax.fori_loop(0, 4, two_chunks, 0)
    phase("down")
    hidden_e = (jax.nn.silu(acc[:, 0:512]) * acc[:, 512:1024]).astype(BF)

    def down_tile(p):
        return dot(hidden_e, ed[:, pl.ds(pl.multiple_of(p * 256, 256), 256)])

    def for_sibling(k, c):
        p = lax.rem(y + 2 + k, 4)
        pair_send[p] = down_tile(2 * p + 1 - core).astype(BF)
        remote(pair_send.at[p], pair_recv.at[p], pair_s.at[p], pair_r.at[p], sibling).start()
        return c
    lax.fori_loop(0, 4, for_sibling, 0)

    def for_own(k, c):
        p = lax.rem(y + 2 + k, 4)
        er_own[p] = down_tile(2 * p + core)
        return c
    lax.fori_loop(0, 4, for_own, 0)

    def pair_sum(p):
        remote(pair_send.at[p], pair_recv.at[p], pair_s.at[p], pair_r.at[p], sibling).wait_recv()
        return er_own[p] + pair_recv[p].astype(F32)

    def to_chips(k, c):
        p = lax.rem(y + 1 + lax.rem(k + 1, 3), 4)
        er_send[p] = pair_sum(p).astype(BF)
        remote(er_send.at[p], er_recv.at[y], er_s.at[p], er_r.at[y], ydev(p)).start()
        return c
    lax.fori_loop(0, 3, to_chips, 0)
    er_own[y] = pair_sum(y)

    phase("yx_wait")
    recv_all(NX, x, xdev, part_y.at[0], lambda p: yx_recv.at[p], yx_s, yx_r)
    summed = yx_recv[0].astype(F32)
    for p in range(1, NX):
        summed = summed + yx_recv[p].astype(F32)
    yz_send[...] = summed.astype(BF).reshape(NZ, 16, 512)
    send_all(NZ, z, zdev, lambda p: yz_send.at[p], yz_recv.at[z], yz_s, yz_r)
    yz_recv[z] = yz_send[z]

    phase("er_wait")
    recv_all(4, y, ydev, er_send.at[0], lambda p: er_recv.at[p], er_s, er_r)
    result = er_own[y]
    for k in range(1, 4):
        result = result + er_recv[lax.rem(y + k, 4)].astype(F32)
    result = result.astype(BF)
    mr_send[...] = (dot(pack[0], result[:, 0:128]) + dot(pack[1], result[:, 128:256])).astype(BF).reshape(NE, 8, 128)
    spread_out(lambda p: mr_send.at[p], mr_recv.at[ep], mr_s, mr_r)
    mr_recv[ep] = mr_send[ep]

    recv_all(NZ, z, zdev, yz_send.at[0], lambda p: yz_recv.at[p], yz_s, yz_r)
    dense = yz_recv[0].astype(F32)
    for p in range(1, NZ):
        dense = dense + yz_recv[p].astype(F32)
    dense = dense * mixing16
    for p in range(NT):
        q, half = p // 2, p % 2
        d5_send[p, 0:4, :] = dense[4 * q : 4 * q + 4, 256 * half : 256 * (half + 1)]
        d5_send[p, 4:8, :] = jnp.zeros((4, 256), F32)
    send_all(NT, t, tdev, lambda p: d5_send.at[p], d5_recv.at[t], d5_s, d5_r)
    d5_recv[t] = d5_send[t]

    phase("d5_wait")
    recv_all(NT, t, tdev, d5_send.at[0], lambda p: d5_recv.at[p], d5_s, d5_r)
    dense_rows = jnp.concatenate([d5_recv[p, 0:4, :] for p in range(NT)], axis=0)
    phase("mr_wait")
    recv_all(NE, ep, edev, mr_send.at[0], lambda p: mr_recv.at[p], mr_s, mr_r)
    returned = mr_recv[...].reshape(256, 128)
    phase("final")
    moe = jnp.concatenate([dot(combine[h], returned) for h in range(2)], axis=1)
    final_v[...] = (middle + moe + dense_rows).astype(BF)

    phase("drain")
    sent_all(NT, t, tdev, lambda p: rs_send.at[p], rs_recv.at[t], rs_s, rs_r)
    sent_all(NT, t, tdev, lambda p: p2_send.at[p], p2_recv.at[t], p2_s, p2_r)
    sent_all(NE, ep, edev, lambda p: md_send.at[p], md_recv.at[ep], md_s, md_r)
    sent_all(NZ, z, zdev, lambda p: rows_x.at[x, z], rows_x.at[x, z], xz_s, xz_r)

    def x_sent(zz, c):
        sent_all(NX, x, xdev, lambda p: rows_x.at[x, zz], rows_x.at[x, zz], xx_s.at[zz], xx_r.at[zz])
        return c
    lax.fori_loop(0, NZ, x_sent, 0)
    from_y(ahead, 0).wait_send()
    from_y(behind, 1).wait_send()
    relayed.wait_send()

    def core_sent(k, c):
        to_sibling(k).wait_send()
        tt = 2 * k + core
        remote(ag_recv.at[tt], ag_recv.at[tt], ac_s.at[k], ag_r.at[tt], sibling).wait_send()
        remote(pair_send.at[k], pair_recv.at[k], pair_s.at[k], pair_r.at[k], sibling).wait_send()
        return c
    lax.fori_loop(0, 4, core_sent, 0)
    sent_all(4, y, ydev, lambda p: own_rows, own_rows, ag_s, ag_r)
    sent_all(NX, x, xdev, lambda p: part_y.at[p], yx_recv.at[x], yx_s, yx_r)
    sent_all(4, y, ydev, lambda p: er_send.at[p], er_recv.at[y], er_s, er_r)
    sent_all(NZ, z, zdev, lambda p: yz_send.at[p], yz_recv.at[z], yz_s, yz_r)
    sent_all(NT, t, tdev, lambda p: d5_send.at[p], d5_recv.at[t], d5_s, d5_r)
    sent_all(NE, ep, edev, lambda p: mr_send.at[p], mr_recv.at[ep], mr_s, mr_r)
    phase(None)


def per_device(*args):
    args = list(args)
    for n in (12, 13, 15, 16):
        args[n] = args[n].T
    inv = jnp.asarray((THETA ** (-np.arange(64) / 64.0)).astype(np.float32)[None, :])
    vmem = pltpu.VMEM

    def dma(*shape):
        return pltpu.SemaphoreType.DMA(shape)

    scratch = [
        vmem((32, 2048), BF), vmem((2048,), BF), vmem((2048, 512), BF), vmem((128,), BF),
        vmem((128, 2048), BF), vmem((32, 128, 128), F32), vmem((32,), jnp.int32), vmem((2048,), BF),
        vmem((2048,), BF), vmem((2, 32), jnp.int32), vmem((2, 32), BF),
        vmem((2048, 512), BF), vmem((2048, 512), BF), vmem((512, 2048), BF), vmem((1, 64), F32),
        vmem((32, 128), F32), vmem((8, 32, 256), BF), vmem((8, 32, 256), BF),
        vmem((8, 8, 256), F32), vmem((8, 8, 256), F32), vmem((4, 8, 16, 512), BF),
        vmem((8, 560, 256), BF), vmem((4, 128, 512), BF), vmem((4, 128, 512), BF),
        vmem((8, 16, 512), BF), vmem((8, 16, 512), BF),
        vmem((32, 8, 128), BF), vmem((32, 8, 128), BF), vmem((8, 128, 256), BF),
        vmem((4, 128, 256), BF), vmem((4, 128, 256), BF), vmem((4, 128, 256), F32),
        vmem((4, 128, 256), BF), vmem((4, 128, 256), BF), vmem((32, 8, 128), BF), vmem((32, 8, 128), BF),
        vmem((8, 8, 256), F32), vmem((8, 8, 256), F32), vmem((128, 1024), F32),
        dma(21),
        dma(8), dma(8), dma(8), dma(8), dma(8), dma(8), dma(8, 4), dma(8, 4), dma(3), dma(4), dma(4), dma(4),
        dma(4), dma(4), dma(8), dma(8),
        dma(32), dma(32), dma(4), dma(8), dma(4), dma(4), dma(4), dma(4), dma(4), dma(32), dma(32), dma(8), dma(8),
    ]
    hbm = pl.BlockSpec(memory_space=pltpu.HBM)
    out = pl.BlockSpec(memory_space=pltpu.VMEM)
    return pl.pallas_call(
        step_kernel,
        out_shape=(
            jax.ShapeDtypeStruct((32, 256), BF),
            jax.ShapeDtypeStruct((32, 1, 128, 128), F32),
        ),
        in_specs=[hbm] * 21,
        out_specs=(out, out),
        scratch_shapes=scratch,
        compiler_params=pltpu.CompilerParams(
            collective_id=0, has_side_effects=True, vmem_limit_bytes=63200 * 1024
        ),
    )(*args, inv)


def solution(mesh):
    in_specs = (
        P("ep", None), P(), P(None, "tp"), P(None, "tp"), P(None, "tp"), P(None, "tp"), P("tp"),
        P("tp", None), P("ep", "tp", None, None), P("ep"), P(), P(), P("tp", "ep"), P("tp", "ep"),
        P("ep", "tp"), P("ep", None), P("ep", None), P("ep", None, "tp"), P("ep", None, "tp"),
        P("ep", "tp", None),
    )
    out_specs = (P("ep", "tp"), P("ep", "tp", None, None))
    return jax.shard_map(per_device, mesh=mesh, in_specs=in_specs, out_specs=out_specs, check_vma=False)
```

time: 74.1 us -> 65.8 us (0.89)
  local copies, waits for them, and re-layouts: 10.5 us -> 4.46 us
  Pallas kernels: 62.8 us -> 60.5 us
    unnamed x6 -> x2, local copies, waits for them, and re-layouts: 10.5 us -> 4.46 us
    pallas_call x1, Pallas kernels: 62.8 us -> 60.5 us  [per_device(): pl.pallas_call(step_kernel, out_shape=(jax.ShapeDtypeStruct((32, 256), BF...]
where the time goes in v2:
time: 65.8 us; the launch traced here: 65.7 us
  Pallas kernels  60.5 us (92%)
  local copies, waits for them, and re-layouts  4.46 us (7%)
    pallas_call x1, Pallas kernels, per_device(): pl.pallas_call(step_kernel, out_shape=(jax.ShapeDtypeStruct((32, 256), BF...  60.5 us
    unnamed x2, local copies, waits for them, and re-layouts  4.46 us

profile of v2, /device:TPU:1, one launch (start us, length us, event | category | flops | bytes accessed | tf_op | source)
XLA Modules:
  0.0 65.7 jit_solution(14018449275839316615)
XLA Ops:
  0.6 60.5 %shard_map.212 = (bf16[32,256]{1,0:T(8,128)(2,1)}, f32[32,1,128,128]{3,2,1,0:T(8,128)}) custom-call(bf16[32,2048]{1,0:T(8,128)(2,1)} %resid_h.1, bf16[2048]{0:T(1024)(128)(2,1)} %norm_gain_h.1, bf16[2048,128]{1,0:T(8,128)(2,1)} %wq_h.1, bf16[2048,128]{1,0:T(8,128)(2,1)} %wk_h.1, bf16[2048,128]{1,0:T(8,128)(2,1)} %wv_h.1, bf16[2048,128]{1,0:T(8,128)(2,1)} %wg_h.1, ...), custom_call_target="tpu_custom_call" | custom-call | tf_op jit(solution)/shard_map/pallas_call | solution.py:527
  61.2 1.3 %copy.25 = bf16[32,256]{1,0:T(8,128)(2,1)} copy(bf16[32,256]{1,0:T(8,128)(2,1)} %get-tuple-element.4) | data formatting | bytes 32768
  62.5 3.1 %copy.26 = f32[32,1,128,128]{3,2,1,0:T(8,128)} copy(f32[32,1,128,128]{3,2,1,0:T(8,128)} %get-tuple-element.5) | data formatting | bytes 4194304

commit v3 on v2

--- a/solution.py
+++ b/solution.py
@@ -40,14 +40,15 @@
 def step_kernel(
     resid_h, norm_gain_h, wq_h, wk_h, wv_h, wg_h, head_gain_h, wo_h, state_h, positions_h,
     ffn_gain_h, w_mix_h, dgate_h, dup_h, ddown_h, routes_h, rweight_h, eg_h, eu_h, ed_h, inv_h,
-    final_v, new_state,
+    final_h, new_state_h,
     resid, norm_gain, wqkvg, head_gain, wo, state, positions, ffn_gain, w_mix,
     routes, rweight, eg, eu, ed, inv,
-    mix, rs_send, rs_recv, p2_send, p2_recv, rows_x, dw, part_y, yx_recv, yz_send, yz_recv,
-    md_send, md_recv, ag_recv, pair_send, pair_recv, er_own, er_send, er_recv, mr_send, mr_recv,
-    d5_send, d5_recv, acc,
-    load_sem,
-    rs_s, rs_r, p2_s, p2_r, xz_s, xz_r, xx_s, xx_r, wy_s, wy_r, wc_s, wc_r, yx_s, yx_r, yz_s, yz_r,
+    mix, rs_send, rs_recv, rr_send, rr_recv, sc_send, sc_recv, sx_send, sx_recv, rows_x, dw,
+    part_y, ry_recv, my_send, yx_recv, yz_send, yz_recv, md_send, md_recv, ag_recv, pair_send, pair_recv, er_own, er_send, er_recv, mr_send, mr_recv,
+    d5_send, d5_recv, acc, final_v,
+    load_sem, out_sem,
+    rs_s, rs_r, rr_s, rr_r, sc_s, sc_r, sx_s, sx_r, xz_s, xz_r, xx_s, xx_r, wy_s, wy_r, wc_s, wc_r,
+    ry_s, ry_r, yx_s, yx_r, yz_s, yz_r,
     md_s, md_r, ag_s, ag_r, ac_s, pair_s, pair_r, er_s, er_r, mr_s, mr_r, d5_s, d5_r,
 ):
     ep = lax.axis_index("ep")
@@ -82,14 +83,6 @@
         if name:
             scope.append(jax.named_scope(name))
             scope[0].__enter__()
-
-    phase("greet")
-    barrier = pltpu.get_barrier_semaphore()
-    for dev, me, n in ((edev, ep, NE), (tdev, t, NT)):
-        def greet(k, c, dev=dev, me=me, n=n):
-            pl.semaphore_signal(barrier, inc=1, device_id=dev(lax.rem(me + k, n)), device_id_type=pl.DeviceIdType.MESH)
-            return c
-        lax.fori_loop(1, n, greet, 0)
 
     loads = {}
     pairs = [
@@ -107,6 +100,15 @@
     for n, (name, src, dst) in enumerate(pairs):
         loads[name] = pltpu.make_async_copy(src, dst, load_sem.at[n])
         loads[name].start()
+
+    phase("greet")
+    barrier = pltpu.get_barrier_semaphore()
+    for dev, me, n in ((edev, ep, NE), (tdev, t, NT)):
+        def greet(k, c, dev=dev, me=me, n=n):
+            p = lax.rem(me + lax.rem(k + n // 2, n - 1) + 1, n)
+            pl.semaphore_signal(barrier, inc=1, device_id=dev(p), device_id_type=pl.DeviceIdType.MESH)
+            return c
+        lax.fori_loop(0, n - 1, greet, 0)
 
     def need(*names):
         for name in names:
@@ -174,24 +176,45 @@
     normed = (mixture - centre) * lax.rsqrt(spread + EPSILON)
     normed = normed * head_gain[...].reshape(1, 128).astype(F32)
     retained = (jax.nn.silu(gating) * normed).astype(BF)
-    partial = dot(retained, wo[...]).astype(BF)
+    partial = dot(retained, wo[...])
     for p in range(NT):
-        rs_send[p] = partial[:, 256 * p : 256 * (p + 1)]
+        rs_send[p] = partial[:, 256 * p : 256 * (p + 1)].astype(BF)
+    for p in range(NT):
+        tile = [partial[4 * p : 4 * p + 4, 512 * q : 512 * (q + 1)] for q in range(4)]
+        rr_send[p] = jnp.concatenate(tile, axis=0).astype(BF)
 
     phase("barrier")
     pl.semaphore_wait(barrier, NE + NT - 2)
 
     phase("rs_send")
     send_all(NT, t, tdev, lambda p: rs_send.at[p], rs_recv.at[t], rs_s, rs_r)
+    send_all(NT, t, tdev, lambda p: rr_send.at[p], rr_recv.at[t], rr_s, rr_r)
     rs_recv[t] = rs_send[t]
+    rr_recv[t] = rr_send[t]
 
     need("ddown", "dgate", "dup")
-    mine = dw.at[t, 0:528]
-    remote(mine, mine, wc_s.at[y], wc_r.at[y], sibling).start()
+    ahead, behind = lax.rem(y + 1, 4), lax.rem(y + 3, 4)
+    onward = lax.rem(y + 1 + 2 * core, 4)
+    origin = lax.rem(y + 3 + 2 * core, 4)
+    across = lax.rem(y + 2, 4)
+    parts = (pl.ds(272, 256), pl.ds(0, 272))
+
+    def weights_to_y(h, owner, slot, target):
+        block = dw.at[2 * owner + core, parts[h]]
+        return remote(block, block, wy_s.at[h, slot], wy_r.at[h, owner], ydev(target))
+
+    def weights_to_sibling(h, owner):
+        block = dw.at[2 * owner + core, parts[h]]
+        return remote(block, block, wc_s.at[h, owner], wc_r.at[h, owner], sibling)
+
+    weights_to_y(0, y, 0, ahead).start()
+    weights_to_y(0, y, 1, behind).start()
+    for h in range(2):
+        weights_to_sibling(h, y).start()
 
     key_t = jnp.transpose(key)
     for s in range(32):
-        new_state[s, 0] = state[s] * decay + key_t[:, s : s + 1] * value[s : s + 1, :]
+        state[s] = state[s] * decay + key_t[:, s : s + 1] * value[s : s + 1, :]
 
     need("routes", "rweight", "ffn_gain", "w_mix")
     ids = jnp.transpose(routes[...].astype(F32))
@@ -216,6 +239,25 @@
     pack = [onehot(pk_row == (pk_col >> 2) * 8 + 4 * h + (pk_col & 3)) for h in range(2)]
     for p in range(NT):
         dw[p, 528:560, :] = jnp.zeros((32, 256), BF)
+    gain_mid = ffn_gain[...].reshape(1, 2048).astype(F32)
+    gain_here = gain_mid[:, 0:256]
+    for p in range(1, NT):
+        gain_here = jnp.where(t == p, gain_mid[:, 256 * p : 256 * (p + 1)], gain_here)
+    mixer = w_mix[...].reshape(1, 2048).astype(F32)
+
+    def as_tile(row):
+        return jnp.concatenate(
+            [jnp.broadcast_to(row[:, 512 * q : 512 * (q + 1)], (4, 512)) for q in range(4)], axis=0
+        )
+
+    gain_tile, mixer_tile = as_tile(gain_mid), as_tile(mixer)
+    pick_row, pick_col = iota((16, 32), 0), iota((16, 32), 1)
+    resid_tile = jnp.zeros((16, 512), F32)
+    for q in range(4):
+        pick = onehot((pick_col == 4 * t + (pick_row & 3)) & ((pick_row >> 2) == q))
+        resid_tile = resid_tile + dot(pick, resid[:, 512 * q : 512 * (q + 1)])
+    new_state_copy = pltpu.make_async_copy(state, new_state_h.at[:, 0], out_sem.at[0])
+    new_state_copy.start()
 
     phase("rs_wait")
     recv_all(NT, t, tdev, rs_send.at[0], lambda p: rs_recv.at[p], rs_s, rs_r)
@@ -225,35 +267,8 @@
     for p in range(1, NT):
         attention = attention + rs_recv[p].astype(F32)
     middle = resid[:, columns].astype(F32) + attention
-    squares = as_row(jnp.sum(middle * middle, axis=-1, keepdims=True), 32)
-    squares = jnp.concatenate([squares, jnp.zeros((1, 224), F32)], axis=1)
-
-    for p in range(NT):
-        p2_send[p, 0:4, :] = middle[4 * p : 4 * p + 4, :]
-        p2_send[p, 4:5, :] = squares
-    send_all(NT, t, tdev, lambda p: p2_send.at[p], p2_recv.at[t], p2_s, p2_r)
-    p2_recv[t] = p2_send[t]
-    ahead, behind = lax.rem(y + 1, 4), lax.rem(y + 3, 4)
-    onward = lax.rem(y + 1 + 2 * core, 4)
-    origin = lax.rem(y + 3 + 2 * core, 4)
-    across = lax.rem(y + 2, 4)
-    remote(mine, mine, wy_s.at[0], wy_r.at[y], ydev(ahead)).start()
-    remote(mine, mine, wy_s.at[1], wy_r.at[y], ydev(behind)).start()
-    phase("p2_wait")
-    recv_all(NT, t, tdev, p2_send.at[0], lambda p: p2_recv.at[p], p2_s, p2_r)
-
-    phase("norms")
-    total = p2_recv[0, 4:5, 0:128]
-    for p in range(1, NT):
-        total = total + p2_recv[p, 4:5, 0:128]
-    scale = lax.rsqrt(as_column(total[:, 0:32], 32) * (1.0 / 2048) + EPSILON)
-    gain_mid = ffn_gain[...].reshape(1, 2048).astype(F32)
-    gain_here = gain_mid[:, 0:256]
-    for p in range(1, NT):
-        gain_here = jnp.where(t == p, gain_mid[:, 256 * p : 256 * (p + 1)], gain_here)
-    normed_mid = (middle * scale * gain_here).astype(BF)
-
-    outgoing = dot(dispatch[0], normed_mid[:, 0:128]) + dot(dispatch[1], normed_mid[:, 128:256])
+    scaled = (middle * gain_here).astype(BF)
+    outgoing = dot(dispatch[0], scaled[:, 0:128]) + dot(dispatch[1], scaled[:, 128:256])
     md_send[...] = outgoing.astype(BF).reshape(NE, 8, 128)
     far = 16
 
@@ -267,20 +282,24 @@
     spread_out(lambda p: md_send.at[p], md_recv.at[ep], md_s, md_r)
     md_recv[ep] = md_send[ep]
 
-    quarters = [
-        jnp.concatenate([p2_recv[2 * q, 0:4, :], p2_recv[2 * q + 1, 0:4, :]], axis=1) for q in range(4)
-    ]
-    sq4 = sum(jnp.sum(v * v, axis=-1, keepdims=True) for v in quarters)
-    scale4 = lax.rsqrt(sq4 * (1.0 / 2048) + EPSILON)
-    mixer = w_mix[...].reshape(1, 2048).astype(F32)
-    rows = [
-        (quarters[q] * scale4 * gain_mid[:, 512 * q : 512 * (q + 1)]).astype(BF).astype(F32) for q in range(4)
-    ]
-    mixing = jax.nn.sigmoid(
-        sum(jnp.sum(rows[q] * mixer[:, 512 * q : 512 * (q + 1)], axis=-1, keepdims=True) for q in range(4))
+    phase("rr_wait")
+    recv_all(NT, t, tdev, rr_send.at[0], lambda p: rr_recv.at[p], rr_s, rr_r)
+    middle_tile = rr_recv[0].astype(F32)
+    for p in range(1, NT):
+        middle_tile = middle_tile + rr_recv[p].astype(F32)
+    middle_tile = middle_tile + resid_tile
+
+    def over_quarters(column):
+        total = column[0:4] + column[4:8] + column[8:12] + column[12:16]
+        return jnp.concatenate([total] * 4, axis=0)
+
+    squares = over_quarters(jnp.sum(middle_tile * middle_tile, axis=-1, keepdims=True))
+    scale_tile = lax.rsqrt(squares * (1.0 / 2048) + EPSILON)
+    normed_tile = (middle_tile * scale_tile * gain_tile).astype(BF)
+    mixing16 = jax.nn.sigmoid(
+        over_quarters(jnp.sum(normed_tile.astype(F32) * mixer_tile, axis=-1, keepdims=True))
     )
-    mixing16 = jnp.concatenate([mixing] * 4, axis=0)
-    rows_x[x, z] = jnp.concatenate(rows, axis=0).astype(BF)
+    rows_x[x, z] = normed_tile
     send_all(NZ, z, zdev, lambda p: rows_x.at[x, z], rows_x.at[x, z], xz_s, xz_r)
 
     def to_x(zz):
@@ -288,23 +307,20 @@
 
     to_x(z)
 
-    phase("relay")
-
-    def weights_of(p):
-        return dw.at[2 * p + core, 0:528]
-
-    def from_y(p, slot):
-        return remote(weights_of(p), weights_of(p), wy_s.at[slot], wy_r.at[p], ydev(p))
-
-    def to_sibling(p):
-        return remote(weights_of(p), weights_of(p), wc_s.at[p], wc_r.at[p], sibling)
-
-    relayed = remote(weights_of(origin), weights_of(origin), wy_s.at[2], wy_r.at[origin], ydev(onward))
-    from_y(origin, 2).wait_recv()
-    relayed.start()
-    to_sibling(origin).start()
-    from_y(onward, 2).wait_recv()
-    to_sibling(onward).start()
+    lane16 = iota((16, 128), 1)
+    sc_send[...] = jnp.sum(jnp.where(lane16 == iota((16, 128), 0), scale_tile, 0.0)[0:4], axis=0, keepdims=True)
+    send_all(NT, t, tdev, lambda p: sc_send, sc_recv.at[t], sc_s, sc_r)
+    sc_recv[t] = sc_send[...]
+    weights_to_y(1, y, 0, ahead).start()
+    weights_to_y(1, y, 1, behind).start()
+
+    def relay(h):
+        weights_to_y(h, origin, 2, onward).wait_recv()
+        weights_to_y(h, origin, 2, onward).start()
+        weights_to_sibling(h, origin).start()
+
+    phase("relay_a")
+    relay(0)
 
     phase("md_wait")
     recv_all(NE, ep, edev, md_send.at[0], lambda p: md_recv.at[p], md_s, md_r)
@@ -327,13 +343,31 @@
         return c
     lax.fori_loop(1, NZ, pass_on, 0)
 
+    phase("relay_b")
+    relay(1)
+
+    phase("sc_wait")
+    recv_all(NT, t, tdev, sc_send, lambda p: sc_recv.at[p], sc_s, sc_r)
+    factors = jnp.concatenate([jnp.broadcast_to(sc_recv[p], (4, 128)) for p in range(NT)], axis=0)
+    factors = jnp.sum(
+        jnp.where(iota((32, 128), 1) == (iota((32, 128), 0) & 3), factors, 0.0), axis=1, keepdims=True
+    )
+    sx_send[...] = jnp.sum(taken * factors, axis=0, keepdims=True)
+    spread_out(lambda p: sx_send, sx_recv.at[ep], sx_s, sx_r)
+    sx_recv[ep] = sx_send[...]
+
     phase("weights_wait")
-    from_y(across, 2).wait_recv()
-    to_sibling(across).start()
+    for h in range(2):
+        weights_to_y(h, onward, 2, onward).wait_recv()
+        weights_to_sibling(h, onward).start()
+    for h in range(2):
+        weights_to_y(h, across, 2, onward).wait_recv()
+        weights_to_sibling(h, across).start()
 
     def all_weights(k, c):
-        theirs = dw.at[2 * k + 1 - core, 0:528]
-        remote(theirs, theirs, wc_s.at[k], wc_r.at[k], sibling).wait_recv()
+        for h in range(2):
+            theirs = dw.at[2 * k + 1 - core, parts[h]]
+            remote(theirs, theirs, wc_s.at[h, k], wc_r.at[h, k], sibling).wait_recv()
         return c
     lax.fori_loop(0, 4, all_weights, 0)
 
@@ -364,10 +398,32 @@
         put = onehot(back_row == (back_col >> 2) * 16 + 4 * q + (back_col & 3))
         packed = packed + dot(put, block)
     part_y[...] = packed.astype(BF).reshape(NX, 128, 512)
-    send_all(NX, x, xdev, lambda p: part_y.at[p], yx_recv.at[x], yx_s, yx_r)
-    yx_recv[x] = part_y[x]
-
-    phase("ag_gate_up")
+    x_on, x_back, x_across = lax.rem(x + 1 + 2 * core, 4), lax.rem(x + 3 + 2 * core, 4), lax.rem(x + 2, 4)
+
+    def half(h):
+        return pl.ds(64 * h, 64)
+
+    def y_across(h):
+        return remote(part_y.at[x_across, half(h)], ry_recv.at[half(h)], ry_s.at[h], ry_r.at[h], xdev(x_on))
+
+    def y_back(h):
+        return remote(part_y.at[x_back, half(h)], yx_recv.at[1, half(h)], yx_s.at[1, h], yx_r.at[1, h], xdev(x_back))
+
+    def y_on(h):
+        return remote(my_send.at[half(h)], yx_recv.at[0, half(h)], yx_s.at[0, h], yx_r.at[0, h], xdev(x_on))
+
+    for h in range(2):
+        y_across(h).start()
+    for h in range(2):
+        y_back(h).start()
+
+    def merge_on():
+        for h in range(2):
+            y_across(h).wait_recv()
+            mine = part_y[x_on, half(h)].astype(F32) + ry_recv[half(h)].astype(F32)
+            my_send[half(h)] = mine.astype(BF)
+            y_on(h).start()
+
     need("eg", "eu", "ed")
 
     def chunk(p):
@@ -392,8 +448,16 @@
         chunk(other)
         return c
     lax.fori_loop(0, 4, two_chunks, 0)
+    phase("merge_on")
+    merge_on()
     phase("down")
-    hidden_e = (jax.nn.silu(acc[:, 0:512]) * acc[:, 512:1024]).astype(BF)
+    recv_all(NE, ep, edev, sx_send, lambda p: sx_recv.at[p], sx_s, sx_r)
+    every = jnp.concatenate([sx_recv[p] for p in range(NE)], axis=0)
+    repeat = jnp.where((iota((128, 32), 0) >> 2) == iota((128, 32), 1), 1.0, 0.0)
+    every = jnp.dot(repeat, every, preferred_element_type=F32, precision=lax.Precision.HIGHEST)
+    wanted = iota((128, 256), 1) == 8 * ep + (iota((128, 256), 0) & 3)
+    factor = jnp.sum(jnp.where(wanted, every, 0.0), axis=1, keepdims=True)
+    hidden_e = (jax.nn.silu(acc[:, 0:512] * factor) * (acc[:, 512:1024] * factor)).astype(BF)
 
     def down_tile(p):
         return dot(hidden_e, ed[:, pl.ds(pl.multiple_of(p * 256, 256), 256)])
@@ -424,13 +488,44 @@
     er_own[y] = pair_sum(y)
 
     phase("yx_wait")
-    recv_all(NX, x, xdev, part_y.at[0], lambda p: yx_recv.at[p], yx_s, yx_r)
-    summed = yx_recv[0].astype(F32)
-    for p in range(1, NX):
-        summed = summed + yx_recv[p].astype(F32)
+    for h in range(2):
+        y_back(h).wait_recv()
+        y_on(h).wait_recv()
+    summed = part_y[x].astype(F32) + yx_recv[0].astype(F32) + yx_recv[1].astype(F32)
     yz_send[...] = summed.astype(BF).reshape(NZ, 16, 512)
     send_all(NZ, z, zdev, lambda p: yz_send.at[p], yz_recv.at[z], yz_s, yz_r)
     yz_recv[z] = yz_send[z]
+
+    phase("drain_early")
+    sent_all(NT, t, tdev, lambda p: rs_send.at[p], rs_recv.at[t], rs_s, rs_r)
+    sent_all(NT, t, tdev, lambda p: rr_send.at[p], rr_recv.at[t], rr_s, rr_r)
+    sent_all(NT, t, tdev, lambda p: sc_send, sc_recv.at[t], sc_s, sc_r)
+    sent_all(NE, ep, edev, lambda p: sx_send, sx_recv.at[ep], sx_s, sx_r)
+    sent_all(NE, ep, edev, lambda p: md_send.at[p], md_recv.at[ep], md_s, md_r)
+    sent_all(NZ, z, zdev, lambda p: rows_x.at[x, z], rows_x.at[x, z], xz_s, xz_r)
+
+    def x_sent(zz, c):
+        sent_all(NX, x, xdev, lambda p: rows_x.at[x, zz], rows_x.at[x, zz], xx_s.at[zz], xx_r.at[zz])
+        return c
+    lax.fori_loop(0, NZ, x_sent, 0)
+    for h in range(2):
+        weights_to_y(h, y, 0, ahead).wait_send()
+        weights_to_y(h, y, 1, behind).wait_send()
+        weights_to_y(h, origin, 2, onward).wait_send()
+        y_across(h).wait_send()
+        y_back(h).wait_send()
+        y_on(h).wait_send()
+
+    def core_sent(k, c):
+        for h in range(2):
+            weights_to_sibling(h, k).wait_send()
+        tt = 2 * k + core
+        remote(ag_recv.at[tt], ag_recv.at[tt], ac_s.at[k], ag_r.at[tt], sibling).wait_send()
+        remote(pair_send.at[k], pair_recv.at[k], pair_s.at[k], pair_r.at[k], sibling).wait_send()
+        return c
+    lax.fori_loop(0, 4, core_sent, 0)
+    sent_all(4, y, ydev, lambda p: own_rows, own_rows, ag_s, ag_r)
+    new_state_copy.wait()
 
     phase("er_wait")
     recv_all(4, y, ydev, er_send.at[0], lambda p: er_recv.at[p], er_s, er_r)
@@ -456,6 +551,8 @@
 
     phase("d5_wait")
     recv_all(NT, t, tdev, d5_send.at[0], lambda p: d5_recv.at[p], d5_s, d5_r)
+    sent_all(4, y, ydev, lambda p: er_send.at[p], er_recv.at[y], er_s, er_r)
+    sent_all(NZ, z, zdev, lambda p: yz_send.at[p], yz_recv.at[z], yz_s, yz_r)
     dense_rows = jnp.concatenate([d5_recv[p, 0:4, :] for p in range(NT)], axis=0)
     phase("mr_wait")
     recv_all(NE, ep, edev, mr_send.at[0], lambda p: mr_recv.at[p], mr_s, mr_r)
@@ -463,35 +560,30 @@
     phase("final")
     moe = jnp.concatenate([dot(combine[h], returned) for h in range(2)], axis=1)
     final_v[...] = (middle + moe + dense_rows).astype(BF)
+    final_copy = pltpu.make_async_copy(final_v, final_h, out_sem.at[1])
+    final_copy.start()
 
     phase("drain")
-    sent_all(NT, t, tdev, lambda p: rs_send.at[p], rs_recv.at[t], rs_s, rs_r)
-    sent_all(NT, t, tdev, lambda p: p2_send.at[p], p2_recv.at[t], p2_s, p2_r)
-    sent_all(NE, ep, edev, lambda p: md_send.at[p], md_recv.at[ep], md_s, md_r)
-    sent_all(NZ, z, zdev, lambda p: rows_x.at[x, z], rows_x.at[x, z], xz_s, xz_r)
-
-    def x_sent(zz, c):
-        sent_all(NX, x, xdev, lambda p: rows_x.at[x, zz], rows_x.at[x, zz], xx_s.at[zz], xx_r.at[zz])
-        return c
-    lax.fori_loop(0, NZ, x_sent, 0)
-    from_y(ahead, 0).wait_send()
-    from_y(behind, 1).wait_send()
-    relayed.wait_send()
-
-    def core_sent(k, c):
-        to_sibling(k).wait_send()
-        tt = 2 * k + core
-        remote(ag_recv.at[tt], ag_recv.at[tt], ac_s.at[k], ag_r.at[tt], sibling).wait_send()
-        remote(pair_send.at[k], pair_recv.at[k], pair_s.at[k], pair_r.at[k], sibling).wait_send()
-        return c
-    lax.fori_loop(0, 4, core_sent, 0)
-    sent_all(4, y, ydev, lambda p: own_rows, own_rows, ag_s, ag_r)
-    sent_all(NX, x, xdev, lambda p: part_y.at[p], yx_recv.at[x], yx_s, yx_r)
-    sent_all(4, y, ydev, lambda p: er_send.at[p], er_recv.at[y], er_s, er_r)
-    sent_all(NZ, z, zdev, lambda p: yz_send.at[p], yz_recv.at[z], yz_s, yz_r)
     sent_all(NT, t, tdev, lambda p: d5_send.at[p], d5_recv.at[t], d5_s, d5_r)
     sent_all(NE, ep, edev, lambda p: mr_send.at[p], mr_recv.at[ep], mr_s, mr_r)
+    final_copy.wait()
     phase(None)
+
+
+def hand_out(final_in, state_in, final_out, state_out, final_v, state_v, in_sem, out_sem):
+    pieces = [(final_in, final_v, final_out)]
+    for n in range(8):
+        part = pl.ds(4 * n, 4)
+        pieces.append((state_in.at[part], state_v.at[part], state_out.at[part]))
+    ins = [pltpu.make_async_copy(a, b, in_sem.at[n]) for n, (a, b, _) in enumerate(pieces)]
+    outs = [pltpu.make_async_copy(b, c, out_sem.at[n]) for n, (_, b, c) in enumerate(pieces)]
+    for copy in ins:
+        copy.start()
+    for copy, out in zip(ins, outs):
+        copy.wait()
+        out.start()
+    for out in outs:
+        out.wait()
 
 
 def per_device(*args):
@@ -510,33 +602,44 @@
         vmem((2048,), BF), vmem((2, 32), jnp.int32), vmem((2, 32), BF),
         vmem((2048, 512), BF), vmem((2048, 512), BF), vmem((512, 2048), BF), vmem((1, 64), F32),
         vmem((32, 128), F32), vmem((8, 32, 256), BF), vmem((8, 32, 256), BF),
-        vmem((8, 8, 256), F32), vmem((8, 8, 256), F32), vmem((4, 8, 16, 512), BF),
-        vmem((8, 560, 256), BF), vmem((4, 128, 512), BF), vmem((4, 128, 512), BF),
+        vmem((8, 16, 512), BF), vmem((8, 16, 512), BF), vmem((1, 128), F32), vmem((8, 1, 128), F32),
+        vmem((1, 256), F32), vmem((32, 1, 256), F32), vmem((4, 8, 16, 512), BF), vmem((8, 560, 256), BF),
+        vmem((4, 128, 512), BF), vmem((128, 512), BF), vmem((128, 512), BF), vmem((2, 128, 512), BF),
         vmem((8, 16, 512), BF), vmem((8, 16, 512), BF),
         vmem((32, 8, 128), BF), vmem((32, 8, 128), BF), vmem((8, 128, 256), BF),
         vmem((4, 128, 256), BF), vmem((4, 128, 256), BF), vmem((4, 128, 256), F32),
         vmem((4, 128, 256), BF), vmem((4, 128, 256), BF), vmem((32, 8, 128), BF), vmem((32, 8, 128), BF),
-        vmem((8, 8, 256), F32), vmem((8, 8, 256), F32), vmem((128, 1024), F32),
-        dma(21),
-        dma(8), dma(8), dma(8), dma(8), dma(8), dma(8), dma(8, 4), dma(8, 4), dma(3), dma(4), dma(4), dma(4),
-        dma(4), dma(4), dma(8), dma(8),
+        vmem((8, 8, 256), F32), vmem((8, 8, 256), F32), vmem((128, 1024), F32), vmem((32, 256), BF),
+        dma(21), dma(2),
+        dma(8), dma(8), dma(8), dma(8), dma(8), dma(8), dma(32), dma(32), dma(8), dma(8), dma(8, 4), dma(8, 4),
+        dma(2, 3), dma(2, 4), dma(2, 4), dma(2, 4), dma(2), dma(2), dma(2, 2), dma(2, 2), dma(8), dma(8),
         dma(32), dma(32), dma(4), dma(8), dma(4), dma(4), dma(4), dma(4), dma(4), dma(32), dma(32), dma(8), dma(8),
     ]
     hbm = pl.BlockSpec(memory_space=pltpu.HBM)
-    out = pl.BlockSpec(memory_space=pltpu.VMEM)
-    return pl.pallas_call(
+    final, new_state = pl.pallas_call(
         step_kernel,
         out_shape=(
             jax.ShapeDtypeStruct((32, 256), BF),
             jax.ShapeDtypeStruct((32, 1, 128, 128), F32),
         ),
         in_specs=[hbm] * 21,
-        out_specs=(out, out),
+        out_specs=(hbm, hbm),
         scratch_shapes=scratch,
         compiler_params=pltpu.CompilerParams(
             collective_id=0, has_side_effects=True, vmem_limit_bytes=63200 * 1024
         ),
     )(*args, inv)
+    return pl.pallas_call(
+        hand_out,
+        out_shape=(
+            jax.ShapeDtypeStruct((32, 256), BF),
+            jax.ShapeDtypeStruct((32, 1, 128, 128), F32),
+        ),
+        in_specs=[hbm, hbm],
+        out_specs=(hbm, hbm),
+        scratch_shapes=[vmem((32, 256), BF), vmem((32, 1, 128, 128), F32), dma(9), dma(9)],
+        compiler_params=pltpu.CompilerParams(vmem_limit_bytes=63200 * 1024),
+    )(final, new_state)
 
 
 def solution(mesh):

time: 65.8 us -> 60.4 us (0.918)
  local copies, waits for them, and re-layouts: 4.46 us -> 0 us
  Pallas kernels: 60.5 us -> 59.6 us
    unnamed x2 -> x0, local copies, waits for them, and re-layouts: 4.46 us -> none
    pallas_call x1, Pallas kernels: 60.5 us -> 57.1 us  [per_device(): pl.pallas_call(step_kernel, out_shape=(jax.ShapeDtypeStruct((32, 256), BF...]
    pallas_call x0 -> x1, Pallas kernels: none -> 2.43 us  [per_device(): pl.pallas_call(hand_out, out_shape=(jax.ShapeDtypeStruct((32, 256), BF),...]
where the time goes in v3:
time: 60.4 us; the launch traced here: 60.2 us
  Pallas kernels  59.6 us (99%)
  between operations  0.65 us (1%)
    pallas_call x1, Pallas kernels, per_device(): pl.pallas_call(step_kernel, out_shape=(jax.ShapeDtypeStruct((32, 256), BF...  57.1 us
    pallas_call x1, Pallas kernels, per_device(): pl.pallas_call(hand_out, out_shape=(jax.ShapeDtypeStruct((32, 256), BF),...  2.43 us

profile of v3, /device:TPU:1, one launch (start us, length us, event | category | flops | bytes accessed | tf_op | source)
XLA Modules:
  0.0 60.2 jit_solution(10253785946822569224)
XLA Ops:
  0.6 57.1 %shard_map.212 = (bf16[32,256]{1,0:T(8,128)(2,1)}, f32[32,1,128,128]{3,2,1,0:T(8,128)}) custom-call(bf16[32,2048]{1,0:T(8,128)(2,1)} %resid_h.1, bf16[2048]{0:T(1024)(128)(2,1)} %norm_gain_h.1, bf16[2048,128]{1,0:T(8,128)(2,1)} %wq_h.1, bf16[2048,128]{1,0:T(8,128)(2,1)} %wk_h.1, bf16[2048,128]{1,0:T(8,128)(2,1)} %wv_h.1, bf16[2048,128]{1,0:T(8,128)(2,1)} %wg_h.1, ...), custom_call_target="tpu_custom_call" | custom-call | tf_op jit(solution)/shard_map/pallas_call | solution.py:619
  57.8 2.4 %shard_map.213 = (bf16[32,256]{1,0:T(8,128)(2,1)}, f32[32,1,128,128]{3,2,1,0:T(8,128)}) custom-call(bf16[32,256]{1,0:T(8,128)(2,1)} %get-tuple-element.4.final_in, f32[32,1,128,128]{3,2,1,0:T(8,128)} %get-tuple-element.5.state_in), custom_call_target="tpu_custom_call" | custom-call | tf_op jit(solution)/shard_map/pallas_call | solution.py:632

commit v4 on v3

--- a/solution.py
+++ b/solution.py
@@ -98,7 +98,8 @@
         ("eg", eg_h.at[0], eg), ("eu", eu_h.at[0], eu), ("ed", ed_h.at[0], ed),
     ]
     for n, (name, src, dst) in enumerate(pairs):
-        loads[name] = pltpu.make_async_copy(src, dst, load_sem.at[n])
+        slot = 2 if name in ("wq", "wk", "wv", "wg") else n
+        loads[name] = pltpu.make_async_copy(src, dst, load_sem.at[slot])
         loads[name].start()
 
     phase("greet")
@@ -123,23 +124,15 @@
     def send_all(n, me, dev, src_at, dst_here, ssem, rsem):
         def one(k, c):
             p = lax.rem(me + k, n)
-            remote(src_at(p), dst_here, ssem.at[p], rsem.at[me], dev(p)).start()
+            remote(src_at(p), dst_here, ssem, rsem, dev(p)).start()
             return c
         lax.fori_loop(1, n, one, 0)
 
-    def recv_all(n, me, dev, src, dst_at, ssem, rsem):
-        def one(k, c):
-            p = lax.rem(me + k, n)
-            remote(src, dst_at(p), ssem.at[p], rsem.at[p], dev(p)).wait_recv()
-            return c
-        lax.fori_loop(1, n, one, 0)
-
-    def sent_all(n, me, dev, src_at, dst, ssem, rsem):
-        def one(k, c):
-            p = lax.rem(me + k, n)
-            remote(src_at(p), dst, ssem.at[p], rsem.at[me], dev(p)).wait_send()
-            return c
-        lax.fori_loop(1, n, one, 0)
+    def arrived_all(block, ssem, rsem):
+        remote(block, block, ssem, rsem, sibling).wait_recv()
+
+    def sent_all(block, ssem, rsem):
+        remote(block, block, ssem, rsem, sibling).wait_send()
 
     phase("retention")
     need("resid", "norm_gain")
@@ -147,7 +140,8 @@
     ms = jnp.mean(res * res, axis=-1, keepdims=True)
     gain_in = norm_gain[...].reshape(1, 2048).astype(F32)
     normed_in = (res * lax.rsqrt(ms + EPSILON) * gain_in).astype(BF)
-    need("positions", "inv", "wq", "wk", "wv", "wg")
+    need("positions", "inv")
+    pltpu.make_async_copy(wqkvg, wqkvg, load_sem.at[2]).wait()
     angles = as_column(positions[...].astype(F32).reshape(1, 32), 32) * inv[...]
     cosine, sine = jnp.cos(angles), jnp.sin(angles)
     cos2 = jnp.concatenate([cosine, cosine], axis=-1)
@@ -199,16 +193,16 @@
     across = lax.rem(y + 2, 4)
     parts = (pl.ds(272, 256), pl.ds(0, 272))
 
-    def weights_to_y(h, owner, slot, target):
+    def weights_to_y(h, owner, target):
         block = dw.at[2 * owner + core, parts[h]]
-        return remote(block, block, wy_s.at[h, slot], wy_r.at[h, owner], ydev(target))
+        return remote(block, block, wy_s, wy_r.at[h, owner], ydev(target))
 
     def weights_to_sibling(h, owner):
         block = dw.at[2 * owner + core, parts[h]]
-        return remote(block, block, wc_s.at[h, owner], wc_r.at[h, owner], sibling)
-
-    weights_to_y(0, y, 0, ahead).start()
-    weights_to_y(0, y, 1, behind).start()
+        return remote(block, block, wc_s, wc_r, sibling)
+
+    weights_to_y(0, y, ahead).start()
+    weights_to_y(0, y, behind).start()
     for h in range(2):
         weights_to_sibling(h, y).start()
 
@@ -260,7 +254,7 @@
     new_state_copy.start()
 
     phase("rs_wait")
-    recv_all(NT, t, tdev, rs_send.at[0], lambda p: rs_recv.at[p], rs_s, rs_r)
+    arrived_all(rs_recv.at[0:7], rs_s, rs_r)
     phase("middle")
     columns = pl.ds(pl.multiple_of(t * 256, 256), 256)
     attention = rs_recv[0].astype(F32)
@@ -275,7 +269,7 @@
     def spread_out(src_at, dst_here, ssem, rsem):
         def one(k, c):
             p = lax.rem(ep + lax.rem(k + far, NE - 1) + 1, NE)
-            remote(src_at(p), dst_here, ssem.at[p], rsem.at[ep], edev(p)).start()
+            remote(src_at(p), dst_here, ssem, rsem, edev(p)).start()
             return c
         lax.fori_loop(0, NE - 1, one, 0)
 
@@ -283,7 +277,7 @@
     md_recv[ep] = md_send[ep]
 
     phase("rr_wait")
-    recv_all(NT, t, tdev, rr_send.at[0], lambda p: rr_recv.at[p], rr_s, rr_r)
+    arrived_all(rr_recv.at[0:7], rr_s, rr_r)
     middle_tile = rr_recv[0].astype(F32)
     for p in range(1, NT):
         middle_tile = middle_tile + rr_recv[p].astype(F32)
@@ -300,10 +294,10 @@
         over_quarters(jnp.sum(normed_tile.astype(F32) * mixer_tile, axis=-1, keepdims=True))
     )
     rows_x[x, z] = normed_tile
-    send_all(NZ, z, zdev, lambda p: rows_x.at[x, z], rows_x.at[x, z], xz_s, xz_r)
+    send_all(NZ, z, zdev, lambda p: rows_x.at[x, z], rows_x.at[x, z], xz_s, xz_r.at[z])
 
     def to_x(zz):
-        send_all(NX, x, xdev, lambda p: rows_x.at[x, zz], rows_x.at[x, zz], xx_s.at[zz], xx_r.at[zz])
+        send_all(NX, x, xdev, lambda p: rows_x.at[x, zz], rows_x.at[x, zz], xx_s, xx_r)
 
     to_x(z)
 
@@ -311,34 +305,31 @@
     sc_send[...] = jnp.sum(jnp.where(lane16 == iota((16, 128), 0), scale_tile, 0.0)[0:4], axis=0, keepdims=True)
     send_all(NT, t, tdev, lambda p: sc_send, sc_recv.at[t], sc_s, sc_r)
     sc_recv[t] = sc_send[...]
-    weights_to_y(1, y, 0, ahead).start()
-    weights_to_y(1, y, 1, behind).start()
+    weights_to_y(1, y, ahead).start()
+    weights_to_y(1, y, behind).start()
 
     def relay(h):
-        weights_to_y(h, origin, 2, onward).wait_recv()
-        weights_to_y(h, origin, 2, onward).start()
+        weights_to_y(h, origin, onward).wait_recv()
+        weights_to_y(h, origin, onward).start()
         weights_to_sibling(h, origin).start()
 
     phase("relay_a")
     relay(0)
 
     phase("md_wait")
-    recv_all(NE, ep, edev, md_send.at[0], lambda p: md_recv.at[p], md_s, md_r)
+    arrived_all(md_recv.at[0:31], md_s, md_r)
     arrived = md_recv[...].reshape(256, 128)
     ag_recv[t] = jnp.concatenate([dot(unpack[h], arrived) for h in range(2)], axis=1).astype(BF)
     own_rows = ag_recv.at[t]
 
-    def group_send(k, c):
-        p = lax.rem(y + 4 - k, 4)
-        remote(own_rows, own_rows, ag_s.at[p], ag_r.at[t], ydev(p)).start()
-        return c
-    lax.fori_loop(1, 4, group_send, 0)
-    remote(own_rows, own_rows, ac_s.at[y], ag_r.at[t], sibling).start()
+    remote(own_rows, own_rows, ag_s, ag_r.at[t], ydev(onward)).start()
+    remote(own_rows, own_rows, ag_s, ag_r.at[t], ydev(origin)).start()
+    remote(own_rows, own_rows, ac_s, ag_r.at[t], sibling).start()
 
     phase("xz_wait")
     def pass_on(k, c):
         p = lax.rem(z + k, NZ)
-        remote(rows_x.at[x, p], rows_x.at[x, p], xz_s.at[p], xz_r.at[p], zdev(p)).wait_recv()
+        remote(rows_x.at[x, p], rows_x.at[x, p], xz_s, xz_r.at[p], zdev(p)).wait_recv()
         to_x(p)
         return c
     lax.fori_loop(1, NZ, pass_on, 0)
@@ -347,7 +338,7 @@
     relay(1)
 
     phase("sc_wait")
-    recv_all(NT, t, tdev, sc_send, lambda p: sc_recv.at[p], sc_s, sc_r)
+    arrived_all(sc_recv.at[0:7], sc_s, sc_r)
     factors = jnp.concatenate([jnp.broadcast_to(sc_recv[p], (4, 128)) for p in range(NT)], axis=0)
     factors = jnp.sum(
         jnp.where(iota((32, 128), 1) == (iota((32, 128), 0) & 3), factors, 0.0), axis=1, keepdims=True
@@ -356,27 +347,56 @@
     spread_out(lambda p: sx_send, sx_recv.at[ep], sx_s, sx_r)
     sx_recv[ep] = sx_send[...]
 
+    need("eg", "eu", "ed")
+
+    def chunk(p):
+        depth = pl.ds(pl.multiple_of(p * 256, 256), 256)
+        rows_p = ag_recv[p]
+        acc[:, 0:512] += dot(rows_p, eg[depth, :])
+        acc[:, 512:1024] += dot(rows_p, eu[depth, :])
+
+    acc[...] = jnp.zeros_like(acc)
+
+    def group_rows(p, ssem, dev):
+        block = ag_recv.at[2 * p + core]
+        return remote(block, block, ssem, ag_r.at[2 * p + core], dev)
+
+    def direct_chunk(p):
+        group_rows(p, ag_s, ydev(p)).wait_recv()
+        group_rows(p, ac_s, sibling).start()
+
+    def other_chunk(p):
+        block = ag_recv.at[2 * p + 1 - core]
+        remote(block, block, ac_s, ag_r.at[2 * p + 1 - core], sibling).wait_recv()
+        chunk(2 * p + 1 - core)
+
+    chunk(t)
+    other_chunk(y)
+    phase("weights_on")
+    for h in range(2):
+        weights_to_y(h, onward, onward).wait_recv()
+        weights_to_sibling(h, onward).start()
+    phase("chunks")
+    direct_chunk(origin)
+    group_rows(origin, ag_s, ydev(onward)).start()
+    chunk(2 * origin + core)
+    direct_chunk(onward)
+    chunk(2 * onward + core)
+    other_chunk(onward)
+    other_chunk(origin)
+    phase("weights_across")
+    for h in range(2):
+        weights_to_y(h, across, onward).wait_recv()
+        weights_to_sibling(h, across).start()
+    phase("last_chunk")
+    direct_chunk(across)
+    chunk(2 * across + core)
+    other_chunk(across)
     phase("weights_wait")
-    for h in range(2):
-        weights_to_y(h, onward, 2, onward).wait_recv()
-        weights_to_sibling(h, onward).start()
-    for h in range(2):
-        weights_to_y(h, across, 2, onward).wait_recv()
-        weights_to_sibling(h, across).start()
-
-    def all_weights(k, c):
-        for h in range(2):
-            theirs = dw.at[2 * k + 1 - core, parts[h]]
-            remote(theirs, theirs, wc_s.at[h, k], wc_r.at[h, k], sibling).wait_recv()
-        return c
-    lax.fori_loop(0, 4, all_weights, 0)
-
-    def rows_in(zz, c):
-        recv_all(NX, x, xdev, rows_x.at[x, zz], lambda p: rows_x.at[p, zz], xx_s.at[zz], xx_r.at[zz])
-        return c
+    arrived_all(dw.at[0:4, 0:528], wc_s, wc_r)
 
     phase("xx_wait")
-    lax.fori_loop(0, NZ, rows_in, 0)
+    arrived_all(rows_x.at[0:3], xx_s, xx_r)
 
     phase("dense_mm")
     tiles = rows_x[...].reshape(512, 512)
@@ -404,13 +424,13 @@
         return pl.ds(64 * h, 64)
 
     def y_across(h):
-        return remote(part_y.at[x_across, half(h)], ry_recv.at[half(h)], ry_s.at[h], ry_r.at[h], xdev(x_on))
+        return remote(part_y.at[x_across, half(h)], ry_recv.at[half(h)], ry_s, ry_r.at[h], xdev(x_on))
 
     def y_back(h):
-        return remote(part_y.at[x_back, half(h)], yx_recv.at[1, half(h)], yx_s.at[1, h], yx_r.at[1, h], xdev(x_back))
+        return remote(part_y.at[x_back, half(h)], yx_recv.at[1, half(h)], yx_s, yx_r, xdev(x_back))
 
     def y_on(h):
-        return remote(my_send.at[half(h)], yx_recv.at[0, half(h)], yx_s.at[0, h], yx_r.at[0, h], xdev(x_on))
+        return remote(my_send.at[half(h)], yx_recv.at[0, half(h)], yx_s, yx_r, xdev(x_on))
 
     for h in range(2):
         y_across(h).start()
@@ -424,34 +444,8 @@
             my_send[half(h)] = mine.astype(BF)
             y_on(h).start()
 
-    need("eg", "eu", "ed")
-
-    def chunk(p):
-        depth = pl.ds(pl.multiple_of(p * 256, 256), 256)
-        rows_p = ag_recv[p]
-        acc[:, 0:512] += dot(rows_p, eg[depth, :])
-        acc[:, 512:1024] += dot(rows_p, eu[depth, :])
-
-    acc[...] = jnp.zeros_like(acc)
-
-    def two_chunks(k, c):
-        p = lax.rem(y + k + k // 2, 4)
-        p = jnp.where(k == 3, across, p)
-        direct, other = 2 * p + core, 2 * p + 1 - core
-
-        @pl.when(k > 0)
-        def _():
-            remote(ag_recv.at[direct], ag_recv.at[direct], ag_s.at[p], ag_r.at[direct], ydev(p)).wait_recv()
-            remote(ag_recv.at[direct], ag_recv.at[direct], ac_s.at[p], ag_r.at[direct], sibling).start()
-        chunk(direct)
-        remote(ag_recv.at[other], ag_recv.at[other], ac_s.at[p], ag_r.at[other], sibling).wait_recv()
-        chunk(other)
-        return c
-    lax.fori_loop(0, 4, two_chunks, 0)
-    phase("merge_on")
-    merge_on()
     phase("down")
-    recv_all(NE, ep, edev, sx_send, lambda p: sx_recv.at[p], sx_s, sx_r)
+    arrived_all(sx_recv.at[0:31], sx_s, sx_r)
     every = jnp.concatenate([sx_recv[p] for p in range(NE)], axis=0)
     repeat = jnp.where((iota((128, 32), 0) >> 2) == iota((128, 32), 1), 1.0, 0.0)
     every = jnp.dot(repeat, every, preferred_element_type=F32, precision=lax.Precision.HIGHEST)
@@ -465,7 +459,7 @@
     def for_sibling(k, c):
         p = lax.rem(y + 2 + k, 4)
         pair_send[p] = down_tile(2 * p + 1 - core).astype(BF)
-        remote(pair_send.at[p], pair_recv.at[p], pair_s.at[p], pair_r.at[p], sibling).start()
+        remote(pair_send.at[p], pair_recv.at[p], pair_s, pair_r.at[p], sibling).start()
         return c
     lax.fori_loop(0, 4, for_sibling, 0)
 
@@ -476,68 +470,62 @@
     lax.fori_loop(0, 4, for_own, 0)
 
     def pair_sum(p):
-        remote(pair_send.at[p], pair_recv.at[p], pair_s.at[p], pair_r.at[p], sibling).wait_recv()
+        remote(pair_send.at[p], pair_recv.at[p], pair_s, pair_r.at[p], sibling).wait_recv()
         return er_own[p] + pair_recv[p].astype(F32)
 
-    def to_chips(k, c):
-        p = lax.rem(y + 1 + lax.rem(k + 1, 3), 4)
-        er_send[p] = pair_sum(p).astype(BF)
-        remote(er_send.at[p], er_recv.at[y], er_s.at[p], er_r.at[y], ydev(p)).start()
-        return c
-    lax.fori_loop(0, 3, to_chips, 0)
+    def group_to(p, target, slot):
+        return remote(er_send.at[p], er_recv.at[slot], er_s, er_r.at[slot], ydev(target))
+
+    er_send[across] = pair_sum(across).astype(BF)
+    group_to(across, onward, 0).start()
+    er_send[origin] = pair_sum(origin).astype(BF)
+    group_to(origin, origin, 1).start()
     er_own[y] = pair_sum(y)
-
+    er_own[onward] = pair_sum(onward)
+
+    def group_merge():
+        group_to(across, onward, 0).wait_recv()
+        er_send[onward] = (er_own[onward] + er_recv[0].astype(F32)).astype(BF)
+        group_to(onward, onward, 2).start()
+
+    phase("merge_on")
+    merge_on()
+    phase("group_merge")
+    group_merge()
     phase("yx_wait")
-    for h in range(2):
-        y_back(h).wait_recv()
-        y_on(h).wait_recv()
+    arrived_all(yx_recv, yx_s, yx_r)
     summed = part_y[x].astype(F32) + yx_recv[0].astype(F32) + yx_recv[1].astype(F32)
     yz_send[...] = summed.astype(BF).reshape(NZ, 16, 512)
     send_all(NZ, z, zdev, lambda p: yz_send.at[p], yz_recv.at[z], yz_s, yz_r)
     yz_recv[z] = yz_send[z]
 
     phase("drain_early")
-    sent_all(NT, t, tdev, lambda p: rs_send.at[p], rs_recv.at[t], rs_s, rs_r)
-    sent_all(NT, t, tdev, lambda p: rr_send.at[p], rr_recv.at[t], rr_s, rr_r)
-    sent_all(NT, t, tdev, lambda p: sc_send, sc_recv.at[t], sc_s, sc_r)
-    sent_all(NE, ep, edev, lambda p: sx_send, sx_recv.at[ep], sx_s, sx_r)
-    sent_all(NE, ep, edev, lambda p: md_send.at[p], md_recv.at[ep], md_s, md_r)
-    sent_all(NZ, z, zdev, lambda p: rows_x.at[x, z], rows_x.at[x, z], xz_s, xz_r)
-
-    def x_sent(zz, c):
-        sent_all(NX, x, xdev, lambda p: rows_x.at[x, zz], rows_x.at[x, zz], xx_s.at[zz], xx_r.at[zz])
-        return c
-    lax.fori_loop(0, NZ, x_sent, 0)
-    for h in range(2):
-        weights_to_y(h, y, 0, ahead).wait_send()
-        weights_to_y(h, y, 1, behind).wait_send()
-        weights_to_y(h, origin, 2, onward).wait_send()
-        y_across(h).wait_send()
-        y_back(h).wait_send()
-        y_on(h).wait_send()
-
-    def core_sent(k, c):
-        for h in range(2):
-            weights_to_sibling(h, k).wait_send()
-        tt = 2 * k + core
-        remote(ag_recv.at[tt], ag_recv.at[tt], ac_s.at[k], ag_r.at[tt], sibling).wait_send()
-        remote(pair_send.at[k], pair_recv.at[k], pair_s.at[k], pair_r.at[k], sibling).wait_send()
-        return c
-    lax.fori_loop(0, 4, core_sent, 0)
-    sent_all(4, y, ydev, lambda p: own_rows, own_rows, ag_s, ag_r)
+    sent_all(rs_recv.at[0:7], rs_s, rs_r)
+    sent_all(rr_recv.at[0:7], rr_s, rr_r)
+    sent_all(sc_recv.at[0:7], sc_s, sc_r)
+    sent_all(sx_recv.at[0:31], sx_s, sx_r)
+    sent_all(md_recv.at[0:31], md_s, md_r)
+    sent_all(rows_x.at[0, 0:7], xz_s, xz_r.at[0])
+
+    sent_all(rows_x.at[0:3], xx_s, xx_r)
+    sent_all(dw.at[0:3, 0:528], wy_s, wy_r.at[0, 0])
+    sent_all(dw.at[0:4, 0:528], wc_s, wc_r)
+    sent_all(ry_recv, ry_s, ry_r.at[0])
+    sent_all(yx_recv, yx_s, yx_r)
+    sent_all(ag_recv.at[0:3], ag_s, ag_r.at[0])
+    sent_all(ag_recv.at[0:4], ac_s, ag_r.at[0])
+    sent_all(pair_send, pair_s, pair_r.at[0])
     new_state_copy.wait()
 
     phase("er_wait")
-    recv_all(4, y, ydev, er_send.at[0], lambda p: er_recv.at[p], er_s, er_r)
-    result = er_own[y]
-    for k in range(1, 4):
-        result = result + er_recv[lax.rem(y + k, 4)].astype(F32)
-    result = result.astype(BF)
+    group_to(origin, origin, 1).wait_recv()
+    group_to(onward, onward, 2).wait_recv()
+    result = (er_own[y] + er_recv[1].astype(F32) + er_recv[2].astype(F32)).astype(BF)
     mr_send[...] = (dot(pack[0], result[:, 0:128]) + dot(pack[1], result[:, 128:256])).astype(BF).reshape(NE, 8, 128)
     spread_out(lambda p: mr_send.at[p], mr_recv.at[ep], mr_s, mr_r)
     mr_recv[ep] = mr_send[ep]
 
-    recv_all(NZ, z, zdev, yz_send.at[0], lambda p: yz_recv.at[p], yz_s, yz_r)
+    arrived_all(yz_recv.at[0:7], yz_s, yz_r)
     dense = yz_recv[0].astype(F32)
     for p in range(1, NZ):
         dense = dense + yz_recv[p].astype(F32)
@@ -550,12 +538,12 @@
     d5_recv[t] = d5_send[t]
 
     phase("d5_wait")
-    recv_all(NT, t, tdev, d5_send.at[0], lambda p: d5_recv.at[p], d5_s, d5_r)
-    sent_all(4, y, ydev, lambda p: er_send.at[p], er_recv.at[y], er_s, er_r)
-    sent_all(NZ, z, zdev, lambda p: yz_send.at[p], yz_recv.at[z], yz_s, yz_r)
+    arrived_all(d5_recv.at[0:7], d5_s, d5_r)
+    sent_all(er_recv.at[0:3], er_s, er_r.at[0])
+    sent_all(yz_recv.at[0:7], yz_s, yz_r)
     dense_rows = jnp.concatenate([d5_recv[p, 0:4, :] for p in range(NT)], axis=0)
     phase("mr_wait")
-    recv_all(NE, ep, edev, mr_send.at[0], lambda p: mr_recv.at[p], mr_s, mr_r)
+    arrived_all(mr_recv.at[0:31], mr_s, mr_r)
     returned = mr_recv[...].reshape(256, 128)
     phase("final")
     moe = jnp.concatenate([dot(combine[h], returned) for h in range(2)], axis=1)
@@ -564,8 +552,8 @@
     final_copy.start()
 
     phase("drain")
-    sent_all(NT, t, tdev, lambda p: d5_send.at[p], d5_recv.at[t], d5_s, d5_r)
-    sent_all(NE, ep, edev, lambda p: mr_send.at[p], mr_recv.at[ep], mr_s, mr_r)
+    sent_all(d5_recv.at[0:7], d5_s, d5_r)
+    sent_all(mr_recv.at[0:31], mr_s, mr_r)
     final_copy.wait()
     phase(None)
 
@@ -595,6 +583,8 @@
 
     def dma(*shape):
         return pltpu.SemaphoreType.DMA(shape)
+
+    one = pltpu.SemaphoreType.DMA
 
     scratch = [
         vmem((32, 2048), BF), vmem((2048,), BF), vmem((2048, 512), BF), vmem((128,), BF),
@@ -611,9 +601,9 @@
         vmem((4, 128, 256), BF), vmem((4, 128, 256), BF), vmem((32, 8, 128), BF), vmem((32, 8, 128), BF),
         vmem((8, 8, 256), F32), vmem((8, 8, 256), F32), vmem((128, 1024), F32), vmem((32, 256), BF),
         dma(21), dma(2),
-        dma(8), dma(8), dma(8), dma(8), dma(8), dma(8), dma(32), dma(32), dma(8), dma(8), dma(8, 4), dma(8, 4),
-        dma(2, 3), dma(2, 4), dma(2, 4), dma(2, 4), dma(2), dma(2), dma(2, 2), dma(2, 2), dma(8), dma(8),
-        dma(32), dma(32), dma(4), dma(8), dma(4), dma(4), dma(4), dma(4), dma(4), dma(32), dma(32), dma(8), dma(8),
+        one, one, one, one, one, one, one, one, one, dma(8), one, one,
+        one, dma(2, 4), one, one, one, dma(2), one, one, one, one,
+        one, one, one, dma(8), one, one, dma(4), one, dma(3), one, one, one, one,
     ]
     hbm = pl.BlockSpec(memory_space=pltpu.HBM)
     final, new_state = pl.pallas_call(

time: 60.4 us -> 56.4 us (0.934)
  Pallas kernels: 59.6 us -> 55.6 us
    pallas_call x1, Pallas kernels: 57.1 us -> 53.2 us  [per_device(): pl.pallas_call(step_kernel, out_shape=(jax.ShapeDtypeStruct((32, 256), BF...]
where the time goes in v4:
time: 56.4 us; the launch traced here: 56.2 us
  Pallas kernels  55.6 us (99%)
  between operations  0.65 us (1%)
    pallas_call x1, Pallas kernels, per_device(): pl.pallas_call(step_kernel, out_shape=(jax.ShapeDtypeStruct((32, 256), BF...  53.2 us
    pallas_call x1, Pallas kernels, per_device(): pl.pallas_call(hand_out, out_shape=(jax.ShapeDtypeStruct((32, 256), BF),...  2.43 us

profile of v4, /device:TPU:1, one launch (start us, length us, event | category | flops | bytes accessed | tf_op | source)
XLA Modules:
  0.0 56.2 jit_solution(18306528723230723089)
XLA Ops:
  0.6 53.2 %shard_map.212 = (bf16[32,256]{1,0:T(8,128)(2,1)}, f32[32,1,128,128]{3,2,1,0:T(8,128)}) custom-call(bf16[32,2048]{1,0:T(8,128)(2,1)} %resid_h.1, bf16[2048]{0:T(1024)(128)(2,1)} %norm_gain_h.1, bf16[2048,128]{1,0:T(8,128)(2,1)} %wq_h.1, bf16[2048,128]{1,0:T(8,128)(2,1)} %wk_h.1, bf16[2048,128]{1,0:T(8,128)(2,1)} %wv_h.1, bf16[2048,128]{1,0:T(8,128)(2,1)} %wg_h.1, ...), custom_call_target="tpu_custom_call" | custom-call | tf_op jit(solution)/shard_map/pallas_call | solution.py:609
  53.8 2.4 %shard_map.213 = (bf16[32,256]{1,0:T(8,128)(2,1)}, f32[32,1,128,128]{3,2,1,0:T(8,128)}) custom-call(bf16[32,256]{1,0:T(8,128)(2,1)} %get-tuple-element.4.final_in, f32[32,1,128,128]{3,2,1,0:T(8,128)} %get-tuple-element.5.state_in), custom_call_target="tpu_custom_call" | custom-call | tf_op jit(solution)/shard_map/pallas_call | solution.py:622

commit v5 on v4

--- a/solution.py
+++ b/solution.py
@@ -44,12 +44,12 @@
     resid, norm_gain, wqkvg, head_gain, wo, state, positions, ffn_gain, w_mix,
     routes, rweight, eg, eu, ed, inv,
     mix, rs_send, rs_recv, rr_send, rr_recv, sc_send, sc_recv, sx_send, sx_recv, rows_x, dw,
-    part_y, ry_recv, my_send, yx_recv, yz_send, yz_recv, md_send, md_recv, ag_recv, pair_send, pair_recv, er_own, er_send, er_recv, mr_send, mr_recv,
-    d5_send, d5_recv, acc, final_v,
+    part_y, ry_recv, my_send, yx_recv, md_send, md_recv, ag_recv, pair_send, pair_recv, er_own, er_send, er_recv, mr_send, mr_recv,
+    zt_send, zt_recv, acc, final_v, rows_a, gate_up,
     load_sem, out_sem,
     rs_s, rs_r, rr_s, rr_r, sc_s, sc_r, sx_s, sx_r, xz_s, xz_r, xx_s, xx_r, wy_s, wy_r, wc_s, wc_r,
-    ry_s, ry_r, yx_s, yx_r, yz_s, yz_r,
-    md_s, md_r, ag_s, ag_r, ac_s, pair_s, pair_r, er_s, er_r, mr_s, mr_r, d5_s, d5_r,
+    ry_s, ry_r, yx_s, yx_r,
+    md_s, md_r, ag_s, ag_r, ac_s, pair_s, pair_r, er_s, er_r, mr_s, mr_r, zt_s, zt_r,
 ):
     ep = lax.axis_index("ep")
     t = lax.axis_index("tp")
@@ -104,12 +104,29 @@
 
     phase("greet")
     barrier = pltpu.get_barrier_semaphore()
-    for dev, me, n in ((edev, ep, NE), (tdev, t, NT)):
-        def greet(k, c, dev=dev, me=me, n=n):
-            p = lax.rem(me + lax.rem(k + n // 2, n - 1) + 1, n)
-            pl.semaphore_signal(barrier, inc=1, device_id=dev(p), device_id_type=pl.DeviceIdType.MESH)
-            return c
-        lax.fori_loop(0, n - 1, greet, 0)
+
+    def greet(dev):
+        pl.semaphore_signal(barrier, inc=1, device_id=dev, device_id_type=pl.DeviceIdType.MESH)
+
+    def greet_column(k, c):
+        for p in range(NT):
+            greet((lax.rem(z + k, NZ) * NX + x, p))
+        return c
+
+    def greet_planes(k, c):
+        for n in range(1, NX):
+            greet((lax.rem(z + k, NZ) * NX + lax.rem(x + n, NX), t))
+        return c
+
+    def greet_group(k, c):
+        greet(tdev(lax.rem(t + k, NT)))
+        return c
+
+    lax.fori_loop(NZ // 2, NZ, greet_column, 0)
+    lax.fori_loop(NZ // 2, NZ, greet_planes, 0)
+    lax.fori_loop(1, NZ // 2, greet_column, 0)
+    lax.fori_loop(0, NZ // 2, greet_planes, 0)
+    lax.fori_loop(1, NT, greet_group, 0)
 
     def need(*names):
         for name in names:
@@ -178,7 +195,7 @@
         rr_send[p] = jnp.concatenate(tile, axis=0).astype(BF)
 
     phase("barrier")
-    pl.semaphore_wait(barrier, NE + NT - 2)
+    pl.semaphore_wait(barrier, NZ * NT - 1 + NZ * (NX - 1))
 
     phase("rs_send")
     send_all(NT, t, tdev, lambda p: rs_send.at[p], rs_recv.at[t], rs_s, rs_r)
@@ -264,14 +281,19 @@
     scaled = (middle * gain_here).astype(BF)
     outgoing = dot(dispatch[0], scaled[:, 0:128]) + dot(dispatch[1], scaled[:, 128:256])
     md_send[...] = outgoing.astype(BF).reshape(NE, 8, 128)
-    far = 16
 
     def spread_out(src_at, dst_here, ssem, rsem):
+        def to(p):
+            remote(src_at(p), dst_here, ssem, rsem, edev(p)).start()
+
         def one(k, c):
-            p = lax.rem(ep + lax.rem(k + far, NE - 1) + 1, NE)
-            remote(src_at(p), dst_here, ssem, rsem, edev(p)).start()
+            for n in range(NX):
+                to(lax.rem(z + k, NZ) * NX + n)
             return c
-        lax.fori_loop(0, NE - 1, one, 0)
+        lax.fori_loop(NZ // 2, NZ, one, 0)
+        lax.fori_loop(1, NZ // 2, one, 0)
+        for n in range(1, NX):
+            to(z * NX + lax.rem(x + n, NX))
 
     spread_out(lambda p: md_send.at[p], md_recv.at[ep], md_s, md_r)
     md_recv[ep] = md_send[ep]
@@ -301,8 +323,9 @@
 
     to_x(z)
 
-    lane16 = iota((16, 128), 1)
-    sc_send[...] = jnp.sum(jnp.where(lane16 == iota((16, 128), 0), scale_tile, 0.0)[0:4], axis=0, keepdims=True)
+    lane4, row4 = iota((4, 128), 1), iota((4, 128), 0)
+    both_factors = jnp.where(lane4 == row4, scale_tile[0:4], 0.0) + jnp.where(lane4 == row4 + 4, mixing16[0:4], 0.0)
+    sc_send[...] = jnp.sum(both_factors, axis=0, keepdims=True)
     send_all(NT, t, tdev, lambda p: sc_send, sc_recv.at[t], sc_s, sc_r)
     sc_recv[t] = sc_send[...]
     weights_to_y(1, y, ahead).start()
@@ -315,6 +338,16 @@
 
     phase("relay_a")
     relay(0)
+
+    phase("xz_near")
+
+    def pass_on(n, c):
+        d = n // 2 + 1
+        p = lax.rem(z + d + lax.rem(n, 2) * (NZ - 2 * d), NZ)
+        remote(rows_x.at[x, p], rows_x.at[x, p], xz_s, xz_r.at[p], zdev(p)).wait_recv()
+        to_x(p)
+        return c
+    lax.fori_loop(0, 2, pass_on, 0)
 
     phase("md_wait")
     arrived_all(md_recv.at[0:31], md_s, md_r)
@@ -327,12 +360,7 @@
     remote(own_rows, own_rows, ac_s, ag_r.at[t], sibling).start()
 
     phase("xz_wait")
-    def pass_on(k, c):
-        p = lax.rem(z + k, NZ)
-        remote(rows_x.at[x, p], rows_x.at[x, p], xz_s, xz_r.at[p], zdev(p)).wait_recv()
-        to_x(p)
-        return c
-    lax.fori_loop(1, NZ, pass_on, 0)
+    lax.fori_loop(2, NZ - 1, pass_on, 0)
 
     phase("relay_b")
     relay(1)
@@ -340,9 +368,9 @@
     phase("sc_wait")
     arrived_all(sc_recv.at[0:7], sc_s, sc_r)
     factors = jnp.concatenate([jnp.broadcast_to(sc_recv[p], (4, 128)) for p in range(NT)], axis=0)
-    factors = jnp.sum(
-        jnp.where(iota((32, 128), 1) == (iota((32, 128), 0) & 3), factors, 0.0), axis=1, keepdims=True
-    )
+    fac_lane, fac_row = iota((32, 128), 1), iota((32, 128), 0) & 3
+    mixing = jnp.sum(jnp.where(fac_lane == fac_row + 4, factors, 0.0), axis=1, keepdims=True)
+    factors = jnp.sum(jnp.where(fac_lane == fac_row, factors, 0.0), axis=1, keepdims=True)
     sx_send[...] = jnp.sum(taken * factors, axis=0, keepdims=True)
     spread_out(lambda p: sx_send, sx_recv.at[ep], sx_s, sx_r)
     sx_recv[ep] = sx_send[...]
@@ -388,61 +416,60 @@
     for h in range(2):
         weights_to_y(h, across, onward).wait_recv()
         weights_to_sibling(h, across).start()
+    phase("ag_across")
+    direct_chunk(across)
+    phase("xx_wait")
+    arrived_all(rows_x.at[0:3], xx_s, xx_r)
+    phase("dense_a")
+    tiles = rows_x[...].reshape(512, 512)
+    spread_row = iota((128, 512), 0)
+    spread_col = iota((128, 512), 1)
+    for q in range(4):
+        take = onehot(spread_col == (spread_row >> 2) * 16 + 4 * q + (spread_row & 3))
+        block = dot(take, tiles).astype(BF)
+        rows_a[2 * q] = block[:, 0:256]
+        rows_a[2 * q + 1] = block[:, 256:512]
+
+    def gate_up_by(side):
+        total = jnp.zeros((128, 384), F32)
+        for p in range(4):
+            n = 2 * p + side
+            total = total + dot_nt(rows_a[n], dw[n, 176:560])
+        return total
+
+    gate_up[...] = gate_up_by(core)
     phase("last_chunk")
-    direct_chunk(across)
     chunk(2 * across + core)
     other_chunk(across)
     phase("weights_wait")
     arrived_all(dw.at[0:4, 0:528], wc_s, wc_r)
-
-    phase("xx_wait")
-    arrived_all(rows_x.at[0:3], xx_s, xx_r)
-
     phase("dense_mm")
-    tiles = rows_x[...].reshape(512, 512)
-    spread_row = iota((128, 512), 0)
-    spread_col = iota((128, 512), 1)
-    gate_up = jnp.zeros((128, 384), F32)
+    both_sums = gate_up[...] + gate_up_by(1 - core)
+    up = pltpu.roll(both_sums, 384 - 176, 1)
+    hidden = jnp.where(iota((128, 256), 1) < 176, jax.nn.silu(both_sums[:, 0:256]) * up[:, 0:256], 0.0).astype(BF)
+    x_on, x_back, x_across = lax.rem(x + 1 + 2 * core, 4), lax.rem(x + 3 + 2 * core, 4), lax.rem(x + 2, 4)
+
+    def y_across(q):
+        return remote(part_y.at[q, x_across], ry_recv.at[q], ry_s, ry_r.at[q], xdev(x_on))
+
+    def y_back(q):
+        return remote(part_y.at[q, x_back], yx_recv.at[1, q], yx_s, yx_r.at[q], xdev(x_back))
+
+    def y_on(q):
+        return remote(my_send.at[q], yx_recv.at[0, q], yx_s, yx_r.at[q], xdev(x_on))
+
     for q in range(4):
-        take = onehot(spread_col == (spread_row >> 2) * 16 + 4 * q + (spread_row & 3))
-        block = dot(take, tiles).astype(BF)
-        gate_up = gate_up + dot_nt(block[:, 0:256], dw[2 * q, 176:560])
-        gate_up = gate_up + dot_nt(block[:, 256:512], dw[2 * q + 1, 176:560])
-    up = pltpu.roll(gate_up, 384 - 176, 1)
-    hidden = jnp.where(iota((128, 256), 1) < 176, jax.nn.silu(gate_up[:, 0:256]) * up[:, 0:256], 0.0).astype(BF)
-    back_row = iota((512, 128), 0)
-    back_col = iota((512, 128), 1)
-    packed = jnp.zeros((512, 512), F32)
-    for q in range(4):
-        block = jnp.concatenate([dot(hidden, dw[2 * q, 0:256]), dot(hidden, dw[2 * q + 1, 0:256])], axis=1).astype(BF)
-        put = onehot(back_row == (back_col >> 2) * 16 + 4 * q + (back_col & 3))
-        packed = packed + dot(put, block)
-    part_y[...] = packed.astype(BF).reshape(NX, 128, 512)
-    x_on, x_back, x_across = lax.rem(x + 1 + 2 * core, 4), lax.rem(x + 3 + 2 * core, 4), lax.rem(x + 2, 4)
-
-    def half(h):
-        return pl.ds(64 * h, 64)
-
-    def y_across(h):
-        return remote(part_y.at[x_across, half(h)], ry_recv.at[half(h)], ry_s, ry_r.at[h], xdev(x_on))
-
-    def y_back(h):
-        return remote(part_y.at[x_back, half(h)], yx_recv.at[1, half(h)], yx_s, yx_r, xdev(x_back))
-
-    def y_on(h):
-        return remote(my_send.at[half(h)], yx_recv.at[0, half(h)], yx_s, yx_r, xdev(x_on))
-
-    for h in range(2):
-        y_across(h).start()
-    for h in range(2):
-        y_back(h).start()
+        for n in range(2):
+            part = dot(hidden, dw[2 * q + n, 0:256]).astype(BF)
+            part_y[q, :, :, 256 * n : 256 * (n + 1)] = part.reshape(NX, 32, 256)
+        y_across(q).start()
+        y_back(q).start()
 
     def merge_on():
-        for h in range(2):
-            y_across(h).wait_recv()
-            mine = part_y[x_on, half(h)].astype(F32) + ry_recv[half(h)].astype(F32)
-            my_send[half(h)] = mine.astype(BF)
-            y_on(h).start()
+        for q in range(4):
+            y_across(q).wait_recv()
+            my_send[q] = (part_y[q, x_on].astype(F32) + ry_recv[q].astype(F32)).astype(BF)
+            y_on(q).start()
 
     phase("down")
     arrived_all(sx_recv.at[0:31], sx_s, sx_r)
@@ -473,31 +500,58 @@
         remote(pair_send.at[p], pair_recv.at[p], pair_s, pair_r.at[p], sibling).wait_recv()
         return er_own[p] + pair_recv[p].astype(F32)
 
-    def group_to(p, target, slot):
-        return remote(er_send.at[p], er_recv.at[slot], er_s, er_r.at[slot], ydev(target))
+    def group_to(p, target, slot, h, sem):
+        part = pl.ds(64 * h, 64)
+        return remote(er_send.at[p, part], er_recv.at[slot, part], er_s, er_r.at[sem], ydev(target))
 
     er_send[across] = pair_sum(across).astype(BF)
-    group_to(across, onward, 0).start()
+    for h in range(2):
+        group_to(across, onward, 0, h, h).start()
     er_send[origin] = pair_sum(origin).astype(BF)
-    group_to(origin, origin, 1).start()
+    for h in range(2):
+        group_to(origin, origin, 1, h, 2).start()
     er_own[y] = pair_sum(y)
     er_own[onward] = pair_sum(onward)
 
     def group_merge():
-        group_to(across, onward, 0).wait_recv()
-        er_send[onward] = (er_own[onward] + er_recv[0].astype(F32)).astype(BF)
-        group_to(onward, onward, 2).start()
+        for h in range(2):
+            group_to(across, onward, 0, h, h).wait_recv()
+            part = pl.ds(64 * h, 64)
+            er_send[onward, part] = (er_own[onward, part] + er_recv[0, part].astype(F32)).astype(BF)
+            group_to(onward, onward, 2, h, 3).start()
 
     phase("merge_on")
     merge_on()
     phase("group_merge")
     group_merge()
     phase("yx_wait")
-    arrived_all(yx_recv, yx_s, yx_r)
-    summed = part_y[x].astype(F32) + yx_recv[0].astype(F32) + yx_recv[1].astype(F32)
-    yz_send[...] = summed.astype(BF).reshape(NZ, 16, 512)
-    send_all(NZ, z, zdev, lambda p: yz_send.at[p], yz_recv.at[z], yz_s, yz_r)
-    yz_recv[z] = yz_send[z]
+    zs_row, zs_col = iota((64, 32), 0), iota((64, 32), 1)
+    to_half = [onehot(zs_row == (zs_col >> 2) * 8 + 4 * h + (zs_col & 3)) for h in range(2)]
+
+    def to_column(p, n):
+        remote(zt_send.at[p, n], zt_recv.at[z * NT + t], zt_s, zt_r, (p * NX + x, n)).start()
+
+    for q in range(4):
+        arrived_all(yx_recv.at[:, q], yx_s, yx_r.at[q])
+        summed = part_y[q, x].astype(F32) + yx_recv[0, q].astype(F32) + yx_recv[1, q].astype(F32)
+        summed = summed.astype(BF)
+        low, high = dot(to_half[0], summed), dot(to_half[1], summed)
+        for n in range(2):
+            tile = low[:, 256 * n : 256 * n + 128] + high[:, 256 * n + 128 : 256 * n + 256]
+            zt_send[:, 2 * q + n] = tile.astype(BF).reshape(NZ, 8, 128)
+
+        def column_out(k, c, q=q):
+            for n in range(2):
+                to_column(lax.rem(z + k, NZ), 2 * q + n)
+            return c
+        lax.fori_loop(NZ // 2, NZ, column_out, 0)
+        lax.fori_loop(1, NZ // 2, column_out, 0)
+
+    def group_out(k, c):
+        to_column(z, lax.rem(t + k, NT))
+        return c
+    lax.fori_loop(1, NT, group_out, 0)
+    zt_recv[z * NT + t] = zt_send[z, t]
 
     phase("drain_early")
     sent_all(rs_recv.at[0:7], rs_s, rs_r)
@@ -511,37 +565,28 @@
     sent_all(dw.at[0:3, 0:528], wy_s, wy_r.at[0, 0])
     sent_all(dw.at[0:4, 0:528], wc_s, wc_r)
     sent_all(ry_recv, ry_s, ry_r.at[0])
-    sent_all(yx_recv, yx_s, yx_r)
+    sent_all(yx_recv, yx_s, yx_r.at[0])
     sent_all(ag_recv.at[0:3], ag_s, ag_r.at[0])
     sent_all(ag_recv.at[0:4], ac_s, ag_r.at[0])
     sent_all(pair_send, pair_s, pair_r.at[0])
     new_state_copy.wait()
 
     phase("er_wait")
-    group_to(origin, origin, 1).wait_recv()
-    group_to(onward, onward, 2).wait_recv()
+    arrived_all(er_recv.at[1], er_s, er_r.at[2])
+    arrived_all(er_recv.at[2], er_s, er_r.at[3])
     result = (er_own[y] + er_recv[1].astype(F32) + er_recv[2].astype(F32)).astype(BF)
     mr_send[...] = (dot(pack[0], result[:, 0:128]) + dot(pack[1], result[:, 128:256])).astype(BF).reshape(NE, 8, 128)
     spread_out(lambda p: mr_send.at[p], mr_recv.at[ep], mr_s, mr_r)
     mr_recv[ep] = mr_send[ep]
 
-    arrived_all(yz_recv.at[0:7], yz_s, yz_r)
-    dense = yz_recv[0].astype(F32)
-    for p in range(1, NZ):
-        dense = dense + yz_recv[p].astype(F32)
-    dense = dense * mixing16
-    for p in range(NT):
-        q, half = p // 2, p % 2
-        d5_send[p, 0:4, :] = dense[4 * q : 4 * q + 4, 256 * half : 256 * (half + 1)]
-        d5_send[p, 4:8, :] = jnp.zeros((4, 256), F32)
-    send_all(NT, t, tdev, lambda p: d5_send.at[p], d5_recv.at[t], d5_s, d5_r)
-    d5_recv[t] = d5_send[t]
-
-    phase("d5_wait")
-    arrived_all(d5_recv.at[0:7], d5_s, d5_r)
+    phase("zt_wait")
+    un_row, un_col = iota((32, 512), 0), iota((32, 512), 1)
+    un_token = ((un_col >> 3) & 7) * 4 + (un_col & 3)
+    gather = [onehot((un_token == un_row) & (((un_col >> 2) & 1) == h)) for h in range(2)]
     sent_all(er_recv.at[0:3], er_s, er_r.at[0])
-    sent_all(yz_recv.at[0:7], yz_s, yz_r)
-    dense_rows = jnp.concatenate([d5_recv[p, 0:4, :] for p in range(NT)], axis=0)
+    arrived_all(zt_recv.at[0:63], zt_s, zt_r)
+    columns_in = zt_recv[...].reshape(512, 128)
+    dense_rows = jnp.concatenate([dot(gather[h], columns_in) for h in range(2)], axis=1) * mixing
     phase("mr_wait")
     arrived_all(mr_recv.at[0:31], mr_s, mr_r)
     returned = mr_recv[...].reshape(256, 128)
@@ -552,7 +597,7 @@
     final_copy.start()
 
     phase("drain")
-    sent_all(d5_recv.at[0:7], d5_s, d5_r)
+    sent_all(zt_recv.at[0:63], zt_s, zt_r)
     sent_all(mr_recv.at[0:31], mr_s, mr_r)
     final_copy.wait()
     phase(None)
@@ -594,16 +639,16 @@
         vmem((32, 128), F32), vmem((8, 32, 256), BF), vmem((8, 32, 256), BF),
         vmem((8, 16, 512), BF), vmem((8, 16, 512), BF), vmem((1, 128), F32), vmem((8, 1, 128), F32),
         vmem((1, 256), F32), vmem((32, 1, 256), F32), vmem((4, 8, 16, 512), BF), vmem((8, 560, 256), BF),
-        vmem((4, 128, 512), BF), vmem((128, 512), BF), vmem((128, 512), BF), vmem((2, 128, 512), BF),
-        vmem((8, 16, 512), BF), vmem((8, 16, 512), BF),
+        vmem((4, 4, 32, 512), BF), vmem((4, 32, 512), BF), vmem((4, 32, 512), BF), vmem((2, 4, 32, 512), BF),
         vmem((32, 8, 128), BF), vmem((32, 8, 128), BF), vmem((8, 128, 256), BF),
         vmem((4, 128, 256), BF), vmem((4, 128, 256), BF), vmem((4, 128, 256), F32),
         vmem((4, 128, 256), BF), vmem((4, 128, 256), BF), vmem((32, 8, 128), BF), vmem((32, 8, 128), BF),
-        vmem((8, 8, 256), F32), vmem((8, 8, 256), F32), vmem((128, 1024), F32), vmem((32, 256), BF),
+        vmem((8, 8, 8, 128), BF), vmem((64, 8, 128), BF), vmem((128, 1024), F32), vmem((32, 256), BF),
+        vmem((8, 128, 256), BF), vmem((128, 384), F32),
         dma(21), dma(2),
         one, one, one, one, one, one, one, one, one, dma(8), one, one,
-        one, dma(2, 4), one, one, one, dma(2), one, one, one, one,
-        one, one, one, dma(8), one, one, dma(4), one, dma(3), one, one, one, one,
+        one, dma(2, 4), one, one, one, dma(4), one, dma(4),
+        one, one, one, dma(8), one, one, dma(4), one, dma(4), one, one, one, one,
     ]
     hbm = pl.BlockSpec(memory_space=pltpu.HBM)
     final, new_state = pl.pallas_call(

time: 56.4 us -> 51.7 us (0.917)
  the two profiles are of different devices: /device:TPU:1 before, /device:TPU:32 now
where the time goes in v5:
time: 51.7 us; the launch traced here: 51.5 us
  Pallas kernels  50.8 us (98%)
  between operations  0.65 us (1%)
    pallas_call x1, Pallas kernels, per_device(): pl.pallas_call(step_kernel, out_shape=(jax.ShapeDtypeStruct((32, 256), BF...  48.4 us
    pallas_call x1, Pallas kernels, per_device(): pl.pallas_call(hand_out, out_shape=(jax.ShapeDtypeStruct((32, 256), BF),...  2.43 us

profile of v5, /device:TPU:32, one launch (start us, length us, event | category | flops | bytes accessed | tf_op | source)
XLA Modules:
  0.0 51.5 jit_solution(11245403499539978638)
XLA Ops:
  0.6 48.4 %shard_map.212 = (bf16[32,256]{1,0:T(8,128)(2,1)}, f32[32,1,128,128]{3,2,1,0:T(8,128)}) custom-call(bf16[32,2048]{1,0:T(8,128)(2,1)} %resid_h.1, bf16[2048]{0:T(1024)(128)(2,1)} %norm_gain_h.1, bf16[2048,128]{1,0:T(8,128)(2,1)} %wq_h.1, bf16[2048,128]{1,0:T(8,128)(2,1)} %wk_h.1, bf16[2048,128]{1,0:T(8,128)(2,1)} %wv_h.1, bf16[2048,128]{1,0:T(8,128)(2,1)} %wg_h.1, ...), custom_call_target="tpu_custom_call" | custom-call | tf_op jit(solution)/shard_map/pallas_call | solution.py:654
  49.1 2.4 %shard_map.213 = (bf16[32,256]{1,0:T(8,128)(2,1)}, f32[32,1,128,128]{3,2,1,0:T(8,128)}) custom-call(bf16[32,256]{1,0:T(8,128)(2,1)} %get-tuple-element.4.final_in, f32[32,1,128,128]{3,2,1,0:T(8,128)} %get-tuple-element.5.state_in), custom_call_target="tpu_custom_call" | custom-call | tf_op jit(solution)/shard_map/pallas_call | solution.py:667

commit v6 on v5

--- a/solution.py
+++ b/solution.py
@@ -49,7 +49,7 @@
     load_sem, out_sem,
     rs_s, rs_r, rr_s, rr_r, sc_s, sc_r, sx_s, sx_r, xz_s, xz_r, xx_s, xx_r, wy_s, wy_r, wc_s, wc_r,
     ry_s, ry_r, yx_s, yx_r,
-    md_s, md_r, ag_s, ag_r, ac_s, pair_s, pair_r, er_s, er_r, mr_s, mr_r, zt_s, zt_r,
+    md_s, md_r, ag_s, ag_r, ah_r, ac_s, pair_s, pair_r, er_s, er_r, mr_s, mr_r, zt_s, zt_r,
 ):
     ep = lax.axis_index("ep")
     t = lax.axis_index("tp")
@@ -355,7 +355,10 @@
     ag_recv[t] = jnp.concatenate([dot(unpack[h], arrived) for h in range(2)], axis=1).astype(BF)
     own_rows = ag_recv.at[t]
 
-    remote(own_rows, own_rows, ag_s, ag_r.at[t], ydev(onward)).start()
+    halves_of = (pl.ds(0, 64), pl.ds(64, 64))
+    for h in range(2):
+        block = ag_recv.at[t, halves_of[h]]
+        remote(block, block, ag_s, ah_r.at[h], ydev(onward)).start()
     remote(own_rows, own_rows, ag_s, ag_r.at[t], ydev(origin)).start()
     remote(own_rows, own_rows, ac_s, ag_r.at[t], sibling).start()
 
@@ -405,8 +408,11 @@
         weights_to_y(h, onward, onward).wait_recv()
         weights_to_sibling(h, onward).start()
     phase("chunks")
-    direct_chunk(origin)
-    group_rows(origin, ag_s, ydev(onward)).start()
+    for h in range(2):
+        block = ag_recv.at[2 * origin + core, halves_of[h]]
+        remote(block, block, ag_s, ah_r.at[h], ydev(origin)).wait_recv()
+        remote(block, block, ag_s, ag_r.at[2 * origin + core], ydev(onward)).start()
+    group_rows(origin, ac_s, sibling).start()
     chunk(2 * origin + core)
     direct_chunk(onward)
     chunk(2 * onward + core)
@@ -438,9 +444,6 @@
         return total
 
     gate_up[...] = gate_up_by(core)
-    phase("last_chunk")
-    chunk(2 * across + core)
-    other_chunk(across)
     phase("weights_wait")
     arrived_all(dw.at[0:4, 0:528], wc_s, wc_r)
     phase("dense_mm")
@@ -471,6 +474,9 @@
             my_send[q] = (part_y[q, x_on].astype(F32) + ry_recv[q].astype(F32)).astype(BF)
             y_on(q).start()
 
+    phase("last_chunk")
+    chunk(2 * across + core)
+    other_chunk(across)
     phase("down")
     arrived_all(sx_recv.at[0:31], sx_s, sx_r)
     every = jnp.concatenate([sx_recv[p] for p in range(NE)], axis=0)
@@ -483,22 +489,14 @@
     def down_tile(p):
         return dot(hidden_e, ed[:, pl.ds(pl.multiple_of(p * 256, 256), 256)])
 
-    def for_sibling(k, c):
-        p = lax.rem(y + 2 + k, 4)
+    for p in (across, onward, y, origin):
         pair_send[p] = down_tile(2 * p + 1 - core).astype(BF)
         remote(pair_send.at[p], pair_recv.at[p], pair_s, pair_r.at[p], sibling).start()
-        return c
-    lax.fori_loop(0, 4, for_sibling, 0)
-
-    def for_own(k, c):
-        p = lax.rem(y + 2 + k, 4)
-        er_own[p] = down_tile(2 * p + core)
-        return c
-    lax.fori_loop(0, 4, for_own, 0)
 
     def pair_sum(p):
+        own = down_tile(2 * p + core)
         remote(pair_send.at[p], pair_recv.at[p], pair_s, pair_r.at[p], sibling).wait_recv()
-        return er_own[p] + pair_recv[p].astype(F32)
+        return own + pair_recv[p].astype(F32)
 
     def group_to(p, target, slot, h, sem):
         part = pl.ds(64 * h, 64)
@@ -648,7 +646,7 @@
         dma(21), dma(2),
         one, one, one, one, one, one, one, one, one, dma(8), one, one,
         one, dma(2, 4), one, one, one, dma(4), one, dma(4),
-        one, one, one, dma(8), one, one, dma(4), one, dma(4), one, one, one, one,
+        one, one, one, dma(8), dma(2), one, one, dma(4), one, dma(4), one, one, one, one,
     ]
     hbm = pl.BlockSpec(memory_space=pltpu.HBM)
     final, new_state = pl.pallas_call(

time: 51.7 us -> 51 us (0.986)
  the two profiles are of different devices: /device:TPU:32 before, /device:TPU:1 now
where the time goes in v6:
time: 51 us; the launch traced here: 50.4 us
  Pallas kernels  49.8 us (98%)
  between operations  0.65 us (1%)
    pallas_call x1, Pallas kernels, per_device(): pl.pallas_call(step_kernel, out_shape=(jax.ShapeDtypeStruct((32, 256), BF...  47.4 us
    pallas_call x1, Pallas kernels, per_device(): pl.pallas_call(hand_out, out_shape=(jax.ShapeDtypeStruct((32, 256), BF),...  2.43 us

profile of v6, /device:TPU:1, one launch (start us, length us, event | category | flops | bytes accessed | tf_op | source)
XLA Modules:
  0.0 50.4 jit_solution(4476448790038291628)
XLA Ops:
  0.6 47.4 %shard_map.212 = (bf16[32,256]{1,0:T(8,128)(2,1)}, f32[32,1,128,128]{3,2,1,0:T(8,128)}) custom-call(bf16[32,2048]{1,0:T(8,128)(2,1)} %resid_h.1, bf16[2048]{0:T(1024)(128)(2,1)} %norm_gain_h.1, bf16[2048,128]{1,0:T(8,128)(2,1)} %wq_h.1, bf16[2048,128]{1,0:T(8,128)(2,1)} %wk_h.1, bf16[2048,128]{1,0:T(8,128)(2,1)} %wv_h.1, bf16[2048,128]{1,0:T(8,128)(2,1)} %wg_h.1, ...), custom_call_target="tpu_custom_call" | custom-call | tf_op jit(solution)/shard_map/pallas_call | solution.py:652
  48.0 2.4 %shard_map.213 = (bf16[32,256]{1,0:T(8,128)(2,1)}, f32[32,1,128,128]{3,2,1,0:T(8,128)}) custom-call(bf16[32,256]{1,0:T(8,128)(2,1)} %get-tuple-element.4.final_in, f32[32,1,128,128]{3,2,1,0:T(8,128)} %get-tuple-element.5.state_in), custom_call_target="tpu_custom_call" | custom-call | tf_op jit(solution)/shard_map/pallas_call | solution.py:665

commit v7 on v6

--- a/solution.py
+++ b/solution.py
@@ -40,13 +40,13 @@
 def step_kernel(
     resid_h, norm_gain_h, wq_h, wk_h, wv_h, wg_h, head_gain_h, wo_h, state_h, positions_h,
     ffn_gain_h, w_mix_h, dgate_h, dup_h, ddown_h, routes_h, rweight_h, eg_h, eu_h, ed_h, inv_h,
-    final_h, new_state_h,
+    final_v, new_state,
     resid, norm_gain, wqkvg, head_gain, wo, state, positions, ffn_gain, w_mix,
     routes, rweight, eg, eu, ed, inv,
     mix, rs_send, rs_recv, rr_send, rr_recv, sc_send, sc_recv, sx_send, sx_recv, rows_x, dw,
     part_y, ry_recv, my_send, yx_recv, md_send, md_recv, ag_recv, pair_send, pair_recv, er_own, er_send, er_recv, mr_send, mr_recv,
-    zt_send, zt_recv, acc, final_v, rows_a, gate_up,
-    load_sem, out_sem,
+    zt_send, zt_recv, acc, rows_a, gate_up,
+    load_sem,
     rs_s, rs_r, rr_s, rr_r, sc_s, sc_r, sx_s, sx_r, xz_s, xz_r, xx_s, xx_r, wy_s, wy_r, wc_s, wc_r,
     ry_s, ry_r, yx_s, yx_r,
     md_s, md_r, ag_s, ag_r, ah_r, ac_s, pair_s, pair_r, er_s, er_r, mr_s, mr_r, zt_s, zt_r,
@@ -225,7 +225,7 @@
 
     key_t = jnp.transpose(key)
     for s in range(32):
-        state[s] = state[s] * decay + key_t[:, s : s + 1] * value[s : s + 1, :]
+        new_state[s, 0] = state[s] * decay + key_t[:, s : s + 1] * value[s : s + 1, :]
 
     need("routes", "rweight", "ffn_gain", "w_mix")
     ids = jnp.transpose(routes[...].astype(F32))
@@ -267,8 +267,6 @@
     for q in range(4):
         pick = onehot((pick_col == 4 * t + (pick_row & 3)) & ((pick_row >> 2) == q))
         resid_tile = resid_tile + dot(pick, resid[:, 512 * q : 512 * (q + 1)])
-    new_state_copy = pltpu.make_async_copy(state, new_state_h.at[:, 0], out_sem.at[0])
-    new_state_copy.start()
 
     phase("rs_wait")
     arrived_all(rs_recv.at[0:7], rs_s, rs_r)
@@ -567,7 +565,6 @@
     sent_all(ag_recv.at[0:3], ag_s, ag_r.at[0])
     sent_all(ag_recv.at[0:4], ac_s, ag_r.at[0])
     sent_all(pair_send, pair_s, pair_r.at[0])
-    new_state_copy.wait()
 
     phase("er_wait")
     arrived_all(er_recv.at[1], er_s, er_r.at[2])
@@ -591,30 +588,22 @@
     phase("final")
     moe = jnp.concatenate([dot(combine[h], returned) for h in range(2)], axis=1)
     final_v[...] = (middle + moe + dense_rows).astype(BF)
-    final_copy = pltpu.make_async_copy(final_v, final_h, out_sem.at[1])
-    final_copy.start()
 
     phase("drain")
     sent_all(zt_recv.at[0:63], zt_s, zt_r)
     sent_all(mr_recv.at[0:31], mr_s, mr_r)
-    final_copy.wait()
     phase(None)
 
 
-def hand_out(final_in, state_in, final_out, state_out, final_v, state_v, in_sem, out_sem):
-    pieces = [(final_in, final_v, final_out)]
+def hand_out(final_v, state_v, final_out, state_out, sem):
+    copies = [pltpu.make_async_copy(final_v, final_out, sem.at[8])]
     for n in range(8):
         part = pl.ds(4 * n, 4)
-        pieces.append((state_in.at[part], state_v.at[part], state_out.at[part]))
-    ins = [pltpu.make_async_copy(a, b, in_sem.at[n]) for n, (a, b, _) in enumerate(pieces)]
-    outs = [pltpu.make_async_copy(b, c, out_sem.at[n]) for n, (_, b, c) in enumerate(pieces)]
-    for copy in ins:
+        copies.append(pltpu.make_async_copy(state_v.at[part], state_out.at[part], sem.at[n]))
+    for copy in copies:
         copy.start()
-    for copy, out in zip(ins, outs):
+    for copy in copies:
         copy.wait()
-        out.start()
-    for out in outs:
-        out.wait()
 
 
 def per_device(*args):
@@ -641,14 +630,17 @@
         vmem((32, 8, 128), BF), vmem((32, 8, 128), BF), vmem((8, 128, 256), BF),
         vmem((4, 128, 256), BF), vmem((4, 128, 256), BF), vmem((4, 128, 256), F32),
         vmem((4, 128, 256), BF), vmem((4, 128, 256), BF), vmem((32, 8, 128), BF), vmem((32, 8, 128), BF),
-        vmem((8, 8, 8, 128), BF), vmem((64, 8, 128), BF), vmem((128, 1024), F32), vmem((32, 256), BF),
+        vmem((8, 8, 8, 128), BF), vmem((64, 8, 128), BF), vmem((128, 1024), F32),
         vmem((8, 128, 256), BF), vmem((128, 384), F32),
-        dma(21), dma(2),
+        dma(21),
         one, one, one, one, one, one, one, one, one, dma(8), one, one,
         one, dma(2, 4), one, one, one, dma(4), one, dma(4),
         one, one, one, dma(8), dma(2), one, one, dma(4), one, dma(4), one, one, one, one,
     ]
     hbm = pl.BlockSpec(memory_space=pltpu.HBM)
+    here = pl.BlockSpec(memory_space=pltpu.VMEM)
+    args = [pltpu.with_memory_space_constraint(a, pltpu.HBM) for a in args]
+    inv = pltpu.with_memory_space_constraint(inv, pltpu.HBM)
     final, new_state = pl.pallas_call(
         step_kernel,
         out_shape=(
@@ -656,10 +648,10 @@
             jax.ShapeDtypeStruct((32, 1, 128, 128), F32),
         ),
         in_specs=[hbm] * 21,
-        out_specs=(hbm, hbm),
+        out_specs=(here, here),
         scratch_shapes=scratch,
         compiler_params=pltpu.CompilerParams(
-            collective_id=0, has_side_effects=True, vmem_limit_bytes=63200 * 1024
+            collective_id=0, has_side_effects=True, vmem_limit_bytes=50000 * 1024
         ),
     )(*args, inv)
     return pl.pallas_call(
@@ -668,10 +660,10 @@
             jax.ShapeDtypeStruct((32, 256), BF),
             jax.ShapeDtypeStruct((32, 1, 128, 128), F32),
         ),
-        in_specs=[hbm, hbm],
+        in_specs=[here, here],
         out_specs=(hbm, hbm),
-        scratch_shapes=[vmem((32, 256), BF), vmem((32, 1, 128, 128), F32), dma(9), dma(9)],
-        compiler_params=pltpu.CompilerParams(vmem_limit_bytes=63200 * 1024),
+        scratch_shapes=[dma(9)],
+        compiler_params=pltpu.CompilerParams(vmem_limit_bytes=16384 * 1024),
     )(final, new_state)
 
 

time: 51 us -> 49.2 us (0.965)
  Pallas kernels: 49.8 us -> 48.1 us
    pallas_call x1, Pallas kernels: 2.43 us -> 1.39 us  [per_device(): pl.pallas_call(hand_out, out_shape=(jax.ShapeDtypeStruct((32, 256), BF),...]
    pallas_call x1, Pallas kernels: 47.4 us -> 46.8 us  [per_device(): pl.pallas_call(step_kernel, out_shape=(jax.ShapeDtypeStruct((32, 256), BF...]
where the time goes in v7:
time: 49.2 us; the launch traced here: 48.8 us
  Pallas kernels  48.1 us (98%)
  between operations  0.65 us (1%)
    pallas_call x1, Pallas kernels, per_device(): pl.pallas_call(step_kernel, out_shape=(jax.ShapeDtypeStruct((32, 256), BF...  46.8 us
    pallas_call x1, Pallas kernels, per_device(): pl.pallas_call(hand_out, out_shape=(jax.ShapeDtypeStruct((32, 256), BF),...  1.39 us

profile of v7, /device:TPU:1, one launch (start us, length us, event | category | flops | bytes accessed | tf_op | source)
XLA Modules:
  0.0 48.8 jit_solution(14805956310897669422)
XLA Ops:
  0.6 46.8 %shard_map.212 = (bf16[32,256]{1,0:T(8,128)(2,1)S(1)}, f32[32,1,128,128]{3,2,1,0:T(8,128)S(1)}) custom-call(bf16[32,2048]{1,0:T(8,128)(2,1)} %resid_h.1, bf16[2048]{0:T(1024)(128)(2,1)} %norm_gain_h.1, bf16[2048,128]{1,0:T(8,128)(2,1)} %wq_h.1, bf16[2048,128]{1,0:T(8,128)(2,1)} %wk_h.1, bf16[2048,128]{1,0:T(8,128)(2,1)} %wv_h.1, bf16[2048,128]{1,0:T(8,128)(2,1)} %wg_h.1, ...), custom_call_target="tpu_custom_call" | custom-call | tf_op jit(solution)/shard_map/pallas_call | solution.py:644
  47.4 1.4 %shard_map.213 = (bf16[32,256]{1,0:T(8,128)(2,1)}, f32[32,1,128,128]{3,2,1,0:T(8,128)}) custom-call(bf16[32,256]{1,0:T(8,128)(2,1)S(1)} %get-tuple-element.4.final_v, f32[32,1,128,128]{3,2,1,0:T(8,128)S(1)} %get-tuple-element.5.state_v), custom_call_target="tpu_custom_call" | custom-call | tf_op jit(solution)/shard_map/pallas_call | solution.py:657

commit v8 on v7

--- a/solution.py
+++ b/solution.py
@@ -98,7 +98,7 @@
         ("eg", eg_h.at[0], eg), ("eu", eu_h.at[0], eu), ("ed", ed_h.at[0], ed),
     ]
     for n, (name, src, dst) in enumerate(pairs):
-        slot = 2 if name in ("wq", "wk", "wv", "wg") else n
+        slot = n if n < 2 else max(2, n - 3)
         loads[name] = pltpu.make_async_copy(src, dst, load_sem.at[slot])
         loads[name].start()
 
@@ -190,15 +190,14 @@
     partial = dot(retained, wo[...])
     for p in range(NT):
         rs_send[p] = partial[:, 256 * p : 256 * (p + 1)].astype(BF)
+    phase("barrier")
+    pl.semaphore_wait(barrier, NZ * NT - 1 + NZ * (NX - 1))
+
+    phase("rs_send")
+    send_all(NT, t, tdev, lambda p: rs_send.at[p], rs_recv.at[t], rs_s, rs_r)
     for p in range(NT):
         tile = [partial[4 * p : 4 * p + 4, 512 * q : 512 * (q + 1)] for q in range(4)]
         rr_send[p] = jnp.concatenate(tile, axis=0).astype(BF)
-
-    phase("barrier")
-    pl.semaphore_wait(barrier, NZ * NT - 1 + NZ * (NX - 1))
-
-    phase("rs_send")
-    send_all(NT, t, tdev, lambda p: rs_send.at[p], rs_recv.at[t], rs_s, rs_r)
     send_all(NT, t, tdev, lambda p: rr_send.at[p], rr_recv.at[t], rr_s, rr_r)
     rs_recv[t] = rs_send[t]
     rr_recv[t] = rr_send[t]
@@ -632,7 +631,7 @@
         vmem((4, 128, 256), BF), vmem((4, 128, 256), BF), vmem((32, 8, 128), BF), vmem((32, 8, 128), BF),
         vmem((8, 8, 8, 128), BF), vmem((64, 8, 128), BF), vmem((128, 1024), F32),
         vmem((8, 128, 256), BF), vmem((128, 384), F32),
-        dma(21),
+        dma(18),
         one, one, one, one, one, one, one, one, one, dma(8), one, one,
         one, dma(2, 4), one, one, one, dma(4), one, dma(4),
         one, one, one, dma(8), dma(2), one, one, dma(4), one, dma(4), one, one, one, one,

time: 49.2 us -> 49.2 us (level)
  no operation moved by 1% of the time
where the time goes in v8:
time: 49.2 us; the launch traced here: 48.8 us
  Pallas kernels  48.1 us (98%)
  between operations  0.65 us (1%)
    pallas_call x1, Pallas kernels, per_device(): pl.pallas_call(step_kernel, out_shape=(jax.ShapeDtypeStruct((32, 256), BF...  46.7 us
    pallas_call x1, Pallas kernels, per_device(): pl.pallas_call(hand_out, out_shape=(jax.ShapeDtypeStruct((32, 256), BF),...  1.39 us

profile of v8, /device:TPU:1, one launch (start us, length us, event | category | flops | bytes accessed | tf_op | source)
XLA Modules:
  0.0 48.8 jit_solution(16662167059156206642)
XLA Ops:
  0.6 46.7 %shard_map.212 = (bf16[32,256]{1,0:T(8,128)(2,1)S(1)}, f32[32,1,128,128]{3,2,1,0:T(8,128)S(1)}) custom-call(bf16[32,2048]{1,0:T(8,128)(2,1)} %resid_h.1, bf16[2048]{0:T(1024)(128)(2,1)} %norm_gain_h.1, bf16[2048,128]{1,0:T(8,128)(2,1)} %wq_h.1, bf16[2048,128]{1,0:T(8,128)(2,1)} %wk_h.1, bf16[2048,128]{1,0:T(8,128)(2,1)} %wv_h.1, bf16[2048,128]{1,0:T(8,128)(2,1)} %wg_h.1, ...), custom_call_target="tpu_custom_call" | custom-call | tf_op jit(solution)/shard_map/pallas_call | solution.py:643
  47.4 1.4 %shard_map.213 = (bf16[32,256]{1,0:T(8,128)(2,1)}, f32[32,1,128,128]{3,2,1,0:T(8,128)}) custom-call(bf16[32,256]{1,0:T(8,128)(2,1)S(1)} %get-tuple-element.4.final_v, f32[32,1,128,128]{3,2,1,0:T(8,128)S(1)} %get-tuple-element.5.state_v), custom_call_target="tpu_custom_call" | custom-call | tf_op jit(solution)/shard_map/pallas_call | solution.py:656
